TPU v7x, 32 devices: a whole 2x2x4 slice. The times are simulated.
32 devices in a mesh: rep: 2 (over y), fs: 4 (over z), tp: 4 (over x, core).
Axes of the slice: x: 2, y: 2, z: 4, core: 2. Of those that a mesh axis runs over, the one named last changes fastest.
Arguments:
- tokens: bfloat16 [2048, 2048], P(('rep', 'fs')), may hold values from -6 to 6
- gate_weight: bfloat16 [2048, 2816], P('fs', 'tp'), may hold values from -0.125 to 0.125
- up_weight: bfloat16 [2048, 2816], P('fs', 'tp'), may hold values from -0.125 to 0.125
- down_weight: bfloat16 [2816, 2048], P('tp', 'fs'), may hold values from -0.109375 to 0.109375
- out_grad: bfloat16 [2048, 2048], P(('rep', 'fs')), may hold values from -6 to 6
Outputs:
- input_grad: bfloat16 [2048, 2048], P(('rep', 'fs'))
- down_grad: float32 [2816, 2048], P('tp', 'fs')
- row_norms: float32 [2816], P('tp')
All inputs are finite; a program needn't handle non-finite values.
Results may differ from a plain program's by a relative error of at most 0.024.
Values may be sent and summed in bfloat16 or wider, within the bound.
No kernel may reach another device: no remote copies, remote signals or barrier semaphores. Data moves between devices by JAX's collectives and lax.ppermute only.
A program may use at most 64 MiB of HBM per device.

v0:
```python
import jax
import jax.numpy as jnp
from jax import lax
from jax.sharding import PartitionSpec as P


def contract_last(left, right):
    return lax.dot_general(
        left, right, (((1,), (1,)), ((), ())), preferred_element_type=jnp.float32
    )


def contract_first(left, right):
    return lax.dot_general(
        left, right, (((0,), (0,)), ((), ())), preferred_element_type=jnp.float32
    )


def on_device(tokens, gate_weight, up_weight, down_weight, out_grad):
    down_full = lax.all_gather(down_weight, "fs", axis=1, tiled=True)
    gate_full, up_full = (
        lax.all_gather(gate_weight, "fs", axis=0, tiled=True),
        lax.all_gather(up_weight, "fs", axis=0, tiled=True),
    )
    gate_pre = jnp.dot(tokens, gate_full, preferred_element_type=jnp.float32)
    up_pre = jnp.dot(tokens, up_full, preferred_element_type=jnp.float32)
    sigma = jax.nn.sigmoid(gate_pre)
    activated = gate_pre * sigma
    hidden = (activated * up_pre).astype(jnp.bfloat16)
    hid_grad = contract_last(out_grad, down_full)
    up_grad = (hid_grad * activated).astype(jnp.bfloat16)
    gate_grad = (hid_grad * up_pre * sigma * (1.0 + gate_pre * (1.0 - sigma))).astype(jnp.bfloat16)
    partial_value = contract_last(gate_grad, gate_full) + contract_last(up_grad, up_full)
    input_grad = lax.psum(partial_value.astype(jnp.bfloat16), "tp")
    columns = lax.all_to_all(out_grad, "fs", split_axis=1, concat_axis=0, tiled=True)
    shard = contract_first(lax.all_gather(hidden, "fs", axis=0, tiled=True), columns)
    shard = lax.psum(shard.astype(jnp.bfloat16), "rep").astype(jnp.float32)
    norms = lax.psum(jnp.sum(shard * shard, axis=1), "fs")
    return (input_grad, shard, norms)


def solution(mesh):
    return jax.shard_map(
        on_device,
        mesh=mesh,
        in_specs=(
            P(("rep", "fs"), None),
            P("fs", "tp"),
            P("fs", "tp"),
            P("tp", "fs"),
            P(("rep", "fs"), None),
        ),
        out_specs=(P(("rep", "fs"), None), P("tp", "fs"), P("tp")),
        check_vma=False,
    )
```

profile of v0, /device:TPU:0, one launch (start us, length us, event | category | flops | bytes accessed | tf_op | source)
XLA Modules:
  0.0 329.1 jit_solution(854777100918134661)
XLA Ops:
  7.2 0.7 all-gather.9.cloned.1.call-update
  8.0 0.7 all-gather.7.cloned.1.call-update
  8.7 0.7 all-gather.5.cloned.1.call-update
  9.4 0.0 all-gather.11.cloned.1.call-start
  9.4 62.0 %all-gather.9.cloned.1.call-done = bf16[2048,704]{0,1:T(8,128)(2,1)} async-done(((bf16[512,704]{0,1:T(8,128)(2,1)}), bf16[2048,704]{0,1:T(8,128)(2,1)}) %all-gather.9.cloned.1.call-update) | async-done | bytes 2883600 | tf_op jit(solution)/shard_map/all_gather | solution.py:22
  71.4 2.8 fusion.8
  74.2 56.6 %all-gather.7.cloned.1.call-done = bf16[2048,704]{0,1:T(8,128)(2,1)} async-done(((bf16[512,704]{0,1:T(8,128)(2,1)}), bf16[2048,704]{0,1:T(8,128)(2,1)}) %all-gather.7.cloned.1.call-update) | async-done | bytes 2883600 | tf_op jit(solution)/shard_map/all_gather | solution.py:23
  130.8 3.7 %multiply_convert_fusion = (bf16[256,704]{0,1:T(8,128)(2,1)}, f32[256,704]{0,1:T(8,128)}) fusion(f32[256,704]{0,1:T(8,128)S(1)} %fusion.8, bf16[256,2048]{1,0:T(8,128)(2,1)S(1)} %copy-done, bf16[2048,704]{0,1:T(8,128)(2,1)} %all-gather.7.cloned.1.call-done), kind=kOutput, calls=%fused_computation.4 | convolution fusion | flops 739278848 | bytes 5734400 | tf_op jit(solution)/shard_map/dot_general | solution.py:26
  134.6 0.0 all-reduce.5.cloned.1.call-start
  134.7 0.5 copy.8
  135.2 56.6 %all_to_all.19 = bf16[256,4,512]{0,2,1:T(8,128)(2,1)S(1)} all-to-all(bf16[256,4,512]{0,2,1:T(8,128)(2,1)S(1)} %bitcast.14), channel_id=1, replica_groups=mesh['rep'=2,'fs'=4,'tp'=4] {'fs'}, dimensions={1} | all-to-all | bytes 2097152 | tf_op jit(solution)/shard_map/all_to_all | solution.py:35
  191.8 0.5 copy.9
  192.4 17.8 %all-gather.5.cloned.1.call-done = bf16[704,2048]{1,0:T(8,128)(2,1)} async-done(((bf16[704,512]{1,0:T(8,128)(2,1)}), bf16[704,2048]{1,0:T(8,128)(2,1)}) %all-gather.5.cloned.1.call-update) | async-done | bytes 2883600 | tf_op jit(solution)/shard_map/all_gather | solution.py:20
  210.1 3.9 %fusion.7 = f32[256,704]{0,1:T(8,128)} fusion(bf16[256,2048]{1,0:T(8,128)(2,1)} %param.9, bf16[704,2048]{1,0:T(8,128)(2,1)} %all-gather.5.cloned.1.call-done), kind=kOutput, calls=%fused_computation.13 | convolution fusion | flops 738197504 | bytes 4653056 | tf_op jit(solution)/shard_map/dot_general | solution.py:8
  214.1 32.2 %all-gather.11.cloned.1.call-done = bf16[1024,704]{0,1:T(8,128)(2,1)} async-done(((bf16[256,704]{0,1:T(8,128)(2,1)}), bf16[1024,704]{0,1:T(8,128)(2,1)}) %all-gather.11.cloned.1.call-update) | async-done | bytes 1441808 | tf_op jit(solution)/shard_map/all_gather | solution.py:36
  246.3 3.2 convolution_convert_fusion
  249.5 0.0 all-reduce.3.cloned.1.call-start
  249.6 3.5 %fusion.2 = f32[256,2048]{1,0:T(8,128)S(1)} fusion(bf16[2048,704]{0,1:T(8,128)(2,1)} %all-gather.9.cloned.1.call-done, f32[256,704]{0,1:T(8,128)S(1)} %copy-done.4, f32[256,704]{0,1:T(8,128)} %fusion.7, f32[256,704]{0,1:T(8,128)} %get-tuple-element.6), kind=kOutput, calls=%fused_computation.9 | convolution fusion | flops 739999744 | bytes 7143424 | tf_op jit(solution)/shard_map/dot_general | solution.py:8
  253.1 2.0 fusion
  255.2 25.6 %all-reduce.5.cloned.1.call-done = bf16[704,512]{1,0:T(8,128)(2,1)} async-done(((bf16[704,512]{1,0:T(8,128)(2,1)}), bf16[704,512]{1,0:T(8,128)(2,1)}) %all-reduce.5.cloned.1.call-update) | async-done | bytes 720912 | tf_op jit(solution)/shard_map/psum | solution.py:37
  280.8 2.3 multiply_reduce_fusion
  283.1 12.2 %psum.23 = f32[704]{0:T(1024)} all-reduce(f32[704]{0:T(1024)S(1)} %get-tuple-element.3), channel_id=1, replica_groups=mesh['rep'=2,'fs'=4,'tp'=4] {'fs'}, use_global_device_ids=true, to_apply=%region_3.0 | all-reduce | flops 704 | bytes 5632 | tf_op jit(solution)/shard_map/psum | solution.py:38
  295.4 24.5 %all-reduce.3.cloned.1.call-done = bf16[256,2048]{1,0:T(8,128)(2,1)} async-done(((bf16[256,2048]{1,0:T(8,128)(2,1)}), bf16[256,2048]{1,0:T(8,128)(2,1)}) %all-reduce.3.cloned.1.call-update) | async-done | bytes 1048592 | tf_op jit(solution)/shard_map/psum | solution.py:34
  319.9 2.3 copy.12
  (18 shorter events, 0.2 us)
Async XLA Ops:
  7.2 64.3 %copy-start = (bf16[256,2048]{1,0:T(8,128)(2,1)S(1)}, bf16[256,2048]{1,0:T(8,128)(2,1)}, u32[]{:S(2)}) copy-start(bf16[256,2048]{1,0:T(8,128)(2,1)} %param.5) | copy-start | bytes 3145732
  7.2 64.2 %all-gather.9.cloned.1.call-start = ((), (), s32[]{:S(2)}) async-start(), calls=%async_computation.3 | async-start | bytes 3604480 | tf_op jit(solution)/shard_map/all_gather | solution.py:22
  7.9 122.9 %all-gather.7.cloned.1.call-start = ((), (), s32[]{:S(2)}) async-start(), calls=%async_computation.2 | async-start | bytes 3604480 | tf_op jit(solution)/shard_map/all_gather | solution.py:23
  8.7 201.5 %all-gather.5.cloned.1.call-start = ((), (), s32[]{:S(2)}) async-start(), calls=%async_computation.1 | async-start | bytes 3604480 | tf_op jit(solution)/shard_map/all_gather | solution.py:20
  9.4 236.9 %all-gather.11.cloned.1.call-start = ((), (), s32[]{:S(2)}) async-start(), calls=%async_computation.5 | async-start | bytes 1802240 | tf_op jit(solution)/shard_map/all_gather | solution.py:36
  74.2 60.4 %copy-start.3 = (f32[256,704]{0,1:T(8,128)}, f32[256,704]{0,1:T(8,128)S(1)}, u32[]{:S(2)}) copy-start(f32[256,704]{0,1:T(8,128)S(1)} %fusion.8) | copy-start | bytes 2162692
  74.2 60.4 %copy-start.2 = (bf16[256,2048]{1,0:T(8,128)(2,1)S(1)}, bf16[256,2048]{1,0:T(8,128)(2,1)}, u32[]{:S(2)}) copy-start(bf16[256,2048]{1,0:T(8,128)(2,1)} %param.9) | copy-start | bytes 3145732
  134.6 146.2 %all-reduce.5.cloned.1.call-start = ((), (), s32[]{:S(2)}) async-start(), calls=%async_computation.6 | async-start | bytes 1441792 | tf_op jit(solution)/shard_map/psum | solution.py:37
  246.3 3.3 %copy-start.4 = (f32[256,704]{0,1:T(8,128)S(1)}, f32[256,704]{0,1:T(8,128)}, u32[]{:S(2)}) copy-start(f32[256,704]{0,1:T(8,128)} %copy-done.3) | copy-start | bytes 2162692
  249.5 70.4 %all-reduce.3.cloned.1.call-start = ((), (), s32[]{:S(2)}) async-start(), calls=%async_computation.4 | async-start | bytes 2097152 | tf_op jit(solution)/shard_map/psum | solution.py:34
  249.6 3.5 %copy-start.1 = (bf16[2048,704]{0,1:T(8,128)(2,1)S(1)}, bf16[2048,704]{0,1:T(8,128)(2,1)}, u32[]{:S(2)}) copy-start(bf16[2048,704]{0,1:T(8,128)(2,1)} %all-gather.7.cloned.1.call-done) | copy-start | bytes 8650756
  249.6 3.5 %copy-start.5 = (f32[256,704]{0,1:T(8,128)S(1)}, f32[256,704]{0,1:T(8,128)}, u32[]{:S(2)}) copy-start(f32[256,704]{0,1:T(8,128)} %fusion.7) | copy-start | bytes 2162692
Sparse Core Ops, SparseCore 0:
  9.6 61.8 all-gather.8
  73.0 57.7 all-gather.6
  132.4 77.6 all-gather.4
  211.6 34.6 all-gather.10
  249.6 31.1 all-reduce.4
  283.6 36.2 all-reduce.2
where the time goes:
time: 329 us
  waiting for transfers between devices  221 us (67%)
  blocking collectives  68.9 us (21%)
  matrix products  19.2 us (6%)
  between operations  14.2 us (4%)
  local copies, waits for them, and re-layouts  3.4 us (1%)
    all_gather x1, waiting for transfers between devices, on_device(): lax.all_gather(gate_weight, 'fs', axis=0, tiled=True)  62 us
    all_to_all x1, blocking collectives, on_device(): lax.all_to_all(out_grad, 'fs', split_axis=1, concat_axis=0, tiled=True)  56.6 us
    all_gather x1, waiting for transfers between devices, on_device(): lax.all_gather(up_weight, 'fs', axis=0, tiled=True)  56.6 us
    all_gather x1, waiting for transfers between devices, on_device(): lax.all_gather(hidden, 'fs', axis=0, tiled=True)  32.2 us
    psum x1, waiting for transfers between devices, on_device(): shard = lax.psum(shard.astype(jnp.bfloat16), 'rep').astype(jnp.float32)  25.6 us
    psum x1, waiting for transfers between devices, on_device(): input_grad = lax.psum(partial_value.astype(jnp.bfloat16), 'tp')  24.5 us
    all_gather x1, waiting for transfers between devices, on_device(): down_full = lax.all_gather(down_weight, 'fs', axis=1, tiled=True)  17.8 us
    psum x1, blocking collectives, on_device(): norms = lax.psum(jnp.sum(shard * shard, axis=1), 'fs')  12.2 us
  transfers between devices with their start and end apart: 6, of which 6 were waited for; matrix products, arithmetic and copies ran while one was open for 6% of the time, Pallas kernels for 0%

commit v1 on v0

v1 whole, which is shorter than its diff:
```python
import jax
import jax.numpy as jnp
from jax import lax
from jax.experimental import pallas as pl
from jax.experimental.pallas import tpu as pltpu
from jax.sharding import PartitionSpec as P


F32, BF16 = jnp.float32, jnp.bfloat16


def contract_last(left, right):
    return lax.dot_general(left, right, (((1,), (1,)), ((), ())), preferred_element_type=F32)


def contract_first(left, right):
    return lax.dot_general(left, right, (((0,), (0,)), ((), ())), preferred_element_type=F32)


def gathered(tokens, gate_weight, up_weight, down_weight, out_grad):
    down_full = lax.all_gather(down_weight, "fs", axis=1, tiled=True)
    gate_full = lax.all_gather(gate_weight, "fs", axis=0, tiled=True)
    up_full = lax.all_gather(up_weight, "fs", axis=0, tiled=True)
    gate_pre = jnp.dot(tokens, gate_full, preferred_element_type=F32)
    up_pre = jnp.dot(tokens, up_full, preferred_element_type=F32)
    hid_grad = contract_last(out_grad, down_full)
    hidden, gate_grad, up_grad = pointwise(gate_pre, up_pre, hid_grad)
    partial_value = contract_last(gate_grad, gate_full) + contract_last(up_grad, up_full)
    input_grad = lax.psum(partial_value.astype(BF16), "tp")
    columns = lax.all_to_all(out_grad, "fs", split_axis=1, concat_axis=0, tiled=True)
    shard = contract_first(lax.all_gather(hidden, "fs", axis=0, tiled=True), columns)
    shard = lax.psum(shard.astype(BF16), "rep").astype(F32)
    norms = lax.psum(jnp.sum(shard * shard, axis=1), "fs")
    return input_grad, shard, norms


def pointwise(gate_pre, up_pre, hid_grad):
    sigma = jax.nn.sigmoid(gate_pre)
    activated = gate_pre * sigma
    hidden = (activated * up_pre).astype(BF16)
    up_grad = (hid_grad * activated).astype(BF16)
    gate_grad = (hid_grad * up_pre * sigma * (1.0 + gate_pre * (1.0 - sigma))).astype(BF16)
    return hidden, gate_grad, up_grad


OUTER_PAIRS = ((0, 1), (1, 0), (2, 3), (3, 2))
INWARD = ((0, 1), (3, 2))
OUTWARD = ((1, 0), (2, 3))
MIDDLE = ((1, 2), (2, 1))
ACROSS = ((0, 3), (3, 0), (1, 2), (2, 1))
SWAP = ((0, 1), (1, 0))
OVER_X = ((0, 2), (2, 0), (1, 3), (3, 1))
OVER_CORE = ((0, 1), (1, 0), (2, 3), (3, 2))


def paired(tokens, gate_weight, up_weight, down_weight, out_grad):
    return paired_body(tokens, gate_weight, up_weight, down_weight, out_grad)


def line_places():
    z = lax.axis_index("fs")
    return z, z + 1 - 2 * (z % 2), jnp.where(z < 2, 2, 1), jnp.where(z < 2, 3, 0)


def is_inner():
    z = lax.axis_index("fs")
    return jnp.logical_and(z > 0, z < 3)


def token_quarters():
    t = lax.axis_index("tp")
    x, c = t // 2, t % 2
    return t, 2 * (1 - x) + c, 2 * x + 1 - c, 3 - t


def call(kernel, outs, scratch=(), flops=0, limit=28):
    def run(*args):
        size = sum(v.size * v.dtype.itemsize for v in args)
        return pl.pallas_call(
            kernel,
            out_shape=outs,
            in_specs=[pl.BlockSpec(memory_space=pltpu.VMEM)] * len(args),
            out_specs=[pl.BlockSpec(memory_space=pltpu.VMEM)] * len(outs),
            scratch_shapes=list(scratch),
            compiler_params=pltpu.CompilerParams(vmem_limit_bytes=limit * 2**20),
            cost_estimate=pl.CostEstimate(flops=flops, bytes_accessed=size, transcendentals=0),
        )(*args)

    return run


def like(shape, dtype):
    return jax.ShapeDtypeStruct(shape, dtype)


def lay_kernel(tok, grad, *refs):
    others, (xs, gs) = refs[:4], refs[4:]
    depth, quarter = xs.shape[2], others[0].shape[1]
    quarters = token_quarters()
    for p, place in enumerate(line_places()):
        cols = pl.ds(pl.multiple_of(place * depth, depth), depth)
        for i in range(4):
            rows = pl.ds(pl.multiple_of(quarters[i] * quarter, quarter), quarter)
            here, there = pl.ds(i * quarter, quarter), pl.ds((4 + i) * quarter, quarter)
            xs[p, here, :] = tok[rows, cols]
            gs[p, here, :] = grad[rows, cols]
            xs[p, there, :] = others[i][0, :, cols]
            gs[p, there, :] = others[i][1, :, cols]


def either(inner, a, b):
    return jnp.where(inner, a[...], b[...])


def dot(a, b):
    return jnp.dot(a, b, preferred_element_type=F32)


def project(ws, cols):
    return sum(contract_last(w, cols[p]) for p, w in enumerate(ws))


def front_kernel(xs, gs, own, pair, mid_i, mid_o, far_i, far_o, pre, near, far, far_cast):
    inner = is_inner()
    part = own.shape[0] // 2
    pre[...] = project((own[...], pair[...], either(inner, mid_i, mid_o), either(inner, far_i, far_o)), xs)
    gate = pre[:part, :]
    hidden = (gate * jax.nn.sigmoid(gate) * pre[part:, :]).astype(BF16)
    near[0] = dot(hidden, gs[0])
    near[1] = dot(hidden, gs[1])
    for p in range(2):
        block = dot(hidden, gs[2 + p])
        far[p] = block
        far_cast[p] = block.astype(BF16)


def pair_kernel(*refs):
    parts, ws, (out,), (cols,) = refs[:8], refs[8:12], refs[12:13], refs[13:]
    quarter, depth = parts[0].shape[0], cols.shape[2]

    @pl.when(is_inner())
    def _():
        for p, place in enumerate(line_places()):
            at = pl.ds(pl.multiple_of(place * depth, depth), depth)
            for i in range(8):
                cols[p, pl.ds(i * quarter, quarter), :] = parts[i][:, at]
        out[...] = project([w[...] for w in ws], cols).astype(BF16)


def back_kernel(gs, d0, d1, d2, d3, got, pre_a, pre_b, *refs):
    weights, (keep, give), (hid,) = (refs[:6], refs[6:12]), refs[12:14], refs[14:]
    inner = is_inner()
    half, count = hid.shape
    part, rows = half // 2, count // 4

    @pl.when(inner)
    def _():
        hid[...] = project((d0[...], d1[...], d2[...], d3[...]), gs)

    @pl.when(jnp.logical_not(inner))
    def _():
        hid[...] = got[...].astype(F32)

    grads = []
    for c, pre in enumerate((pre_a, pre_b)):
        _, gate_grad, up_grad = pointwise(pre[:part, :], pre[part:, :], hid[c * part:(c + 1) * part, :])
        grads.append(jnp.concatenate([gate_grad, up_grad], 0))
    width = keep.shape[-1]
    for p in range(4):
        total = None
        for c in range(2):
            own, pair, mid_i, mid_o, far_i, far_o = weights[c]
            w = (own[...], pair[...])[p] if p < 2 else either(inner, *((mid_i, mid_o), (far_i, far_o))[p - 2])
            term = contract_first(grads[c], w)
            total = term if total is None else total + term
        total = total.astype(BF16)
        at = pl.ds((p % 2) * (width // 2), width // 2)
        for group in range(2):
            base = group * 2 * rows
            keep[p // 2, group, :, at] = total[base:base + rows]
            give[p // 2, group, :, at] = total[base + rows:base + 2 * rows]


def place_kernel(*refs):
    parts, out = refs[:4], refs[4]
    quarters, places = token_quarters(), line_places()
    rows, width = parts[0].shape
    quarter, depth = rows // 2, width // 2
    for p in range(4):
        cols = pl.ds(pl.multiple_of(places[p] * depth, depth), depth)
        for i in range(4):
            at = pl.ds(pl.multiple_of(quarters[i] * quarter, quarter), quarter)
            source = parts[2 * (i // 2) + p // 2]
            out[at, cols] = source[(i % 2) * quarter:(i % 2 + 1) * quarter, (p % 2) * depth:(p % 2 + 1) * depth]


def paired_body(tokens, gate_weight, up_weight, down_weight, out_grad):
    y, t = lax.axis_index("rep"), lax.axis_index("tp")
    rows, width = tokens.shape
    units, depth = down_weight.shape
    half, quarter = units // 2, rows // 4
    part, count = half // 2, 2 * rows

    def my_part(w, c):
        return lax.dynamic_slice_in_dim(w, y * half + c * part, part, 0)

    gate_t, up_t = gate_weight.T, up_weight.T
    gu = [jnp.concatenate([my_part(gate_t, c), my_part(up_t, c)], 0) for c in range(2)]
    down_h = lax.dynamic_slice_in_dim(down_weight, y * half, half, 0)
    mine = [lax.dynamic_slice_in_dim(a, t * quarter, quarter, 0) for a in (tokens, out_grad)]

    p1a = lax.ppermute(gu[0], "fs", OUTER_PAIRS)
    p2a = lax.ppermute(gu[0], "fs", MIDDLE)
    p1b = lax.ppermute(gu[1], "fs", OUTER_PAIRS)
    p2b = lax.ppermute(gu[1], "fs", MIDDLE)
    q0 = lax.ppermute(jnp.stack(mine, 0), "rep", SWAP)
    p1d = lax.ppermute(down_h, "fs", INWARD)
    gp = [None] * 8
    gp[0] = lax.ppermute(mine[1], "fs", INWARD)
    p3a = lax.ppermute(p1a, "fs", MIDDLE)
    p4a = lax.ppermute(p2a, "fs", OUTWARD)
    p3b = lax.ppermute(p1b, "fs", MIDDLE)
    p4b = lax.ppermute(p2b, "fs", OUTWARD)
    q1 = lax.ppermute(q0, "tp", OVER_X)
    p2d = lax.ppermute(down_h, "fs", MIDDLE)
    q2 = lax.ppermute(q0, "tp", OVER_CORE)
    p5a = lax.ppermute(p3a, "fs", OUTWARD)
    p3d = lax.ppermute(p1d, "fs", MIDDLE)
    q3 = lax.ppermute(q1, "tp", OVER_CORE)
    gp[4] = lax.ppermute(gp[0], "rep", SWAP)
    p5b = lax.ppermute(p3b, "fs", OUTWARD)
    gp_x = lax.ppermute(jnp.stack([gp[0], gp[4]], 0), "tp", OVER_X)
    gp[1], gp[5] = gp_x[0], gp_x[1]
    for j in (0, 1, 4, 5):
        gp[j + 2] = lax.ppermute(gp[j], "tp", OVER_CORE)

    stacked = like((4, count, depth), BF16)
    xs, gs = call(lay_kernel, [stacked, stacked])(tokens, out_grad, q0, q1, q2, q3)
    gu_sets = ((gu[0], p1a, p2a, p4a, p3a, p5a), (gu[1], p1b, p2b, p4b, p3b, p5b))
    fronts = []
    for c in range(2):
        outs = [like((half, count), F32)] + [like((2, part, depth), d) for d in (F32, F32, BF16)]
        fronts.append(call(front_kernel, outs, flops=2 * count * width * (half + part))(xs, gs, *gu_sets[c]))
    gots = []
    for c in range(2):
        got = lax.ppermute(fronts[c][3], "fs", INWARD)
        gots.append((fronts[c][2] + got.astype(F32)).astype(BF16))

    down_pieces = (down_h, p1d, p2d, p3d)
    (pair_hid,) = call(
        pair_kernel, [like((half, count), BF16)], [pltpu.VMEM((4, count, depth), BF16)], flops=2 * count * width * half
    )(*gp, *down_pieces)
    hid_got = lax.ppermute(pair_hid, "fs", OUTWARD)

    gots = [lax.ppermute(gots[c], "fs", MIDDLE).astype(F32) for c in range(2)]
    keep, give = call(
        back_kernel,
        [like((2, 2, rows // 2, width // 2), BF16)] * 2,
        [pltpu.VMEM((half, count), F32)],
        flops=6 * count * width * half,
    )(gs, *down_pieces, hid_got, fronts[0][0], fronts[1][0], *gu_sets[0], *gu_sets[1])
    got = lax.ppermute(give, "tp", OVER_CORE)
    halved = (keep.astype(F32) + got.astype(F32)).astype(BF16)

    finals = []
    for c in range(2):
        near = fronts[c][1]
        last = lax.ppermute((near[1] + gots[c][1]).astype(BF16), "fs", OUTER_PAIRS).astype(F32)
        finals.append((near[0] + gots[c][0] + last).astype(BF16))
    peers = [lax.ppermute(finals[c], "rep", SWAP) for c in range(2)]
    final_own, peers = jnp.concatenate(finals, 0), jnp.concatenate(peers, 0)
    low = jnp.where(y == 0, final_own, peers)
    high = jnp.where(y == 0, peers, final_own)
    down_grad = jnp.concatenate([low, high], 0).astype(F32)
    wide = final_own.astype(F32)
    norm = jnp.sum(wide * wide, axis=1, keepdims=True).reshape(1, half)
    norm = norm + lax.ppermute(norm, "fs", OUTER_PAIRS)
    norm = norm + lax.ppermute(norm, "fs", ACROSS)
    norm_peer = lax.ppermute(norm, "rep", SWAP)
    norms = jnp.concatenate([jnp.where(y == 0, norm, norm_peer), jnp.where(y == 0, norm_peer, norm)], 1).reshape(units)

    done = []
    for i in range(2):
        got = lax.ppermute(halved[i, 1], "rep", SWAP)
        mine = (halved[i, 0].astype(F32) + got.astype(F32)).astype(BF16)
        got = lax.ppermute(mine, "tp", OVER_X)
        flipped = jnp.concatenate([got[quarter:], got[:quarter]], 0)
        done.append((mine.astype(F32) + flipped.astype(F32)).astype(BF16))
    done += [lax.ppermute(done[i], "tp", OVER_CORE) for i in range(2)]
    (input_grad,) = call(place_kernel, [like((rows, width), BF16)])(*done)
    return input_grad, down_grad, norms


def solution(mesh):
    sizes = dict(mesh.shape)
    line = (sizes["rep"], sizes["fs"], sizes["tp"]) == (2, 4, 4)
    return jax.shard_map(
        paired if line else gathered,
        mesh=mesh,
        in_specs=(
            P(("rep", "fs"), None),
            P("fs", "tp"),
            P("fs", "tp"),
            P("tp", "fs"),
            P(("rep", "fs"), None),
        ),
        out_specs=(P(("rep", "fs"), None), P("tp", "fs"), P("tp")),
        check_vma=False,
    )
```

time: 329 us -> 170 us (0.52)
  waiting for transfers between devices: 221 us -> 88.5 us
  blocking collectives: 68.9 us -> 0 us
  starting transfers between devices: 0.24 us -> 67 us
  matrix products: 19.2 us -> 0 us
  between operations: 14.2 us -> 1.21 us
  Pallas kernels: 0 us -> 6.71 us
    all_gather x4 -> x0, waiting for transfers between devices: 169 us -> none  [the longest x1 62 us: on_device(): lax.all_gather(gate_weight, 'fs', axis=0, tiled=True)]
    ppermute x0 -> x43, waiting for transfers between devices: none -> 88.5 us  [the longest x1 21.4 us: paired_body(): p4b = lax.ppermute(p2b, 'fs', OUTWARD)]
    ppermute x0 -> x43, starting transfers between devices: none -> 67 us  [the longest x2 19.3 us: paired_body(): lax.ppermute((near[1] + gots[c][1]).astype(BF16), 'fs', OUTER_PAIRS)]
    all_to_all x1 -> x0, blocking collectives: 56.6 us -> none  [on_device(): lax.all_to_all(out_grad, 'fs', split_axis=1, concat_axis=0, tiled=True)]
    psum x2 -> x0, waiting for transfers between devices: 50.1 us -> none  [the longest x1 25.6 us: on_device(): shard = lax.psum(shard.astype(jnp.bfloat16), 'rep').astype(jnp.float32)]
    dot_general x6 -> x0, matrix products: 19.2 us -> none  [the longest x3 9.5 us: contract_last(): lax.dot_general(left, right, (((1,), (1,)), ((), ())), preferred_element_...]
    psum x1 -> x0, blocking collectives: 12.2 us -> none  [on_device(): norms = lax.psum(jnp.sum(shard * shard, axis=1), 'fs')]
    pallas_call x0 -> x6, Pallas kernels: none -> 6.71 us  [run(): pl.pallas_call(kernel, out_shape=outs, in_specs=[pl.BlockSpec(memory_spac...]
  transfers between devices with their start and end apart: 6 -> 43, of which waited for: 6 -> 18; matrix products, arithmetic and copies ran while one was open for 6% -> 2% of each run, Pallas kernels for 0% -> 3%
where the time goes in v1:
time: 170 us
  waiting for transfers between devices  88.5 us (52%)
  starting transfers between devices  67 us (39%)
  Pallas kernels  6.71 us (4%)
  other arithmetic  3.79 us (2%)
  local copies, waits for them, and re-layouts  2.39 us (1%)
    ppermute x1, waiting for transfers between devices, paired_body(): p4b = lax.ppermute(p2b, 'fs', OUTWARD)  21.4 us
    ppermute x2, starting transfers between devices, paired_body(): lax.ppermute((near[1] + gots[c][1]).astype(BF16), 'fs', OUTER_PAIRS)  19.3 us
    ppermute x1, waiting for transfers between devices, paired_body(): gp[0] = lax.ppermute(mine[1], 'fs', INWARD)  9.03 us
    ppermute x1, waiting for transfers between devices, paired_body(): gp_x = lax.ppermute(jnp.stack([gp[0], gp[4]], 0), 'tp', OVER_X)  8.13 us
    ppermute x1, waiting for transfers between devices, paired_body(): p5b = lax.ppermute(p3b, 'fs', OUTWARD)  7.72 us
    ppermute x1, waiting for transfers between devices, paired_body(): p5a = lax.ppermute(p3a, 'fs', OUTWARD)  7.72 us
    pallas_call x6, Pallas kernels, run(): pl.pallas_call(kernel, out_shape=outs, in_specs=[pl.BlockSpec(memory_spac...  6.71 us
    ppermute x1, starting transfers between devices, paired_body(): p1a = lax.ppermute(gu[0], 'fs', OUTER_PAIRS)  5.35 us
  transfers between devices with their start and end apart: 43, of which 18 were waited for; matrix products, arithmetic and copies ran while one was open for 2% of the time, Pallas kernels for 3%

profile of v1, /device:TPU:0, one launch (start us, length us, event | category | flops | bytes accessed | tf_op | source)
XLA Modules:
  0.0 169.6 jit_solution(8426310390339173573)
XLA Ops:
  0.7 2.1 %dynamic-slice_bitcast_fusion.1 = (bf16[176,512]{1,0:T(8,128)(2,1)S(1)}, bf16[176,512]{1,0:T(8,128)(2,1)}, bf16[176,512]{1,0:T(8,128)(2,1)}, bf16[176,512]{1,0:T(8,128)(2,1)S(1)}) fusion(bf16[512,704]{0,1:T(8,128)(2,1)} %param.7, s32[]{:T(128)S(6)} %select_n.39, s32[]{:T(128)S(6)} %select_n.38, bf16[512,704]{0,1:T(8,128)(2,1)} %param.6), kind=kLoop, calls=%fused_computation.39 | loop fusion | bytes 1441800 | tf_op jit(solution)/shard_map/dynamic_slice | solution.py:205
  2.8 3.1 %collective-permute-start.20 = (bf16[352,512]{1,0:T(8,128)(2,1)S(1)}, bf16[352,512]{1,0:T(8,128)(2,1)S(1)}, u32[]{:S(2)}, u32[]{:S(2)}) collective-permute-start(bf16[352,512]{1,0:T(8,128)(2,1)S(1)} %pad_maximum_fusion.3.own.refs_6_), channel_id=1, source_target_pairs={{0,4},{4,0},{8,12},{12,8},{1,5},{5,1},{9,13},{13,9},{2,6},{6,2},{1... | collective-permute-start | bytes 1081352 | tf_op jit(solution)/shard_map/ppermute | solution.py:214
  6.0 2.1 %collective-permute-start.7 = (bf16[64,2048]{1,0:T(8,128)(2,1)S(1)}, bf16[64,2048]{1,0:T(8,128)(2,1)S(1)}, u32[]{:S(2)}, u32[]{:S(2)}) collective-permute-start(bf16[64,2048]{1,0:T(8,128)(2,1)S(1)} %constant_dynamic-slice_fusion.1), channel_id=1, source_target_pairs={{0,4},{12,8},{1,5},{13,9},{2,6},{14,10},{3,7},{15,11},{16,20},{28,... | collective-permute-start | bytes 786440 | tf_op jit(solution)/shard_map/ppermute | solution.py:219
  8.2 2.0 %collective-permute-start = (bf16[2,64,2048]{2,1,0:T(8,128)(2,1)S(1)}, bf16[2,64,2048]{2,1,0:T(8,128)(2,1)S(1)}, u32[]{:S(2)}, u32[]{:S(2)}) collective-permute-start(bf16[2,64,2048]{2,1,0:T(8,128)(2,1)S(1)} %pad_maximum_fusion), channel_id=1, source_target_pairs={{0,16},{16,0},{1,17},{17,1},{2,18},{18,2},{3,19},{19,3},{4,20},{20... | collective-permute-start | bytes 1572872 | tf_op jit(solution)/shard_map/ppermute | solution.py:216
  10.2 9.0 %collective-permute-done.7.refs_0_ = bf16[64,2048]{1,0:T(8,128)(2,1)S(1)} collective-permute-done((bf16[64,2048]{1,0:T(8,128)(2,1)S(1)}, bf16[64,2048]{1,0:T(8,128)(2,1)S(1)}, u32[]{:S(2)}, u32[]{:S(2)}) %collective-permute-start.7) | collective-permute-done | bytes 262176 | tf_op jit(solution)/shard_map/ppermute | solution.py:219
  21.5 5.3 %collective-permute-start.15 = (bf16[352,512]{1,0:T(8,128)(2,1)S(1)}, bf16[352,512]{1,0:T(8,128)(2,1)S(1)}, u32[]{:S(2)}, u32[]{:S(2)}) collective-permute-start(bf16[352,512]{1,0:T(8,128)(2,1)S(1)} %pad_maximum_fusion.2.own.refs_0_), channel_id=1, source_target_pairs={{0,4},{4,0},{8,12},{12,8},{1,5},{5,1},{9,13},{13,9},{2,6},{6,2},{1... | collective-permute-start | bytes 1081352 | tf_op jit(solution)/shard_map/ppermute | solution.py:212
  27.6 3.6 %collective-permute-start.4 = (bf16[352,512]{1,0:T(8,128)(2,1)S(1)}, bf16[352,512]{1,0:T(8,128)(2,1)S(1)}, u32[]{:S(2)}, u32[]{:S(2)}) collective-permute-start(bf16[352,512]{1,0:T(8,128)(2,1)S(1)} %constant_dynamic-slice_fusion.refs_8_.d0), channel_id=1, source_target_pairs={{0,4},{12,8},{1,5},{13,9},{2,6},{14,10},{3,7},{15,11},{16,20},{28,... | collective-permute-start | bytes 1081352 | tf_op jit(solution)/shard_map/ppermute | solution.py:217
  33.4 2.3 %collective-permute-done.15.pair.refs_1_ = bf16[352,512]{1,0:T(8,128)(2,1)S(1)} collective-permute-done((bf16[352,512]{1,0:T(8,128)(2,1)S(1)}, bf16[352,512]{1,0:T(8,128)(2,1)S(1)}, u32[]{:S(2)}, u32[]{:S(2)}) %collective-permute-start.15) | collective-permute-done | bytes 360480 | tf_op jit(solution)/shard_map/ppermute | solution.py:212
  37.0 3.8 %collective-permute-done.4.refs_9_.d1 = bf16[352,512]{1,0:T(8,128)(2,1)S(1)} collective-permute-done((bf16[352,512]{1,0:T(8,128)(2,1)S(1)}, bf16[352,512]{1,0:T(8,128)(2,1)S(1)}, u32[]{:S(2)}, u32[]{:S(2)}) %collective-permute-start.4) | collective-permute-done | bytes 360480 | tf_op jit(solution)/shard_map/ppermute | solution.py:217
  43.2 2.9 %collective-permute-done.1.refs_1_ = bf16[2,64,2048]{2,1,0:T(8,128)(2,1)S(1)} collective-permute-done((bf16[2,64,2048]{2,1,0:T(8,128)(2,1)S(1)}, bf16[2,64,2048]{2,1,0:T(8,128)(2,1)S(1)}, u32[]{:S(2)}, u32[]{:S(2)}) %collective-permute-start.1) | collective-permute-done | bytes 524320 | tf_op jit(solution)/shard_map/ppermute | solution.py:224
  46.1 8.1 %collective-permute-done.9 = bf16[2,64,2048]{2,1,0:T(8,128)(2,1)S(1)} collective-permute-done((bf16[2,64,2048]{2,1,0:T(8,128)(2,1)S(1)}, bf16[2,64,2048]{2,1,0:T(8,128)(2,1)S(1)}, u32[]{:S(2)}, u32[]{:S(2)}) %collective-permute-start.9) | collective-permute-done | bytes 524320 | tf_op jit(solution)/shard_map/ppermute | solution.py:232
  61.9 21.4 %collective-permute-done.22.mid_o.refs_9_ = bf16[352,512]{1,0:T(8,128)(2,1)S(1)} collective-permute-done((bf16[352,512]{1,0:T(8,128)(2,1)S(1)}, bf16[352,512]{1,0:T(8,128)(2,1)S(1)}, u32[]{:S(2)}, u32[]{:S(2)}) %collective-permute-start.22) | collective-permute-done | bytes 360480 | tf_op jit(solution)/shard_map/ppermute | solution.py:223
  83.3 7.7 %collective-permute-done.24.far_o.refs_11_ = bf16[352,512]{1,0:T(8,128)(2,1)S(1)} collective-permute-done((bf16[352,512]{1,0:T(8,128)(2,1)S(1)}, bf16[352,512]{1,0:T(8,128)(2,1)S(1)}, u32[]{:S(2)}, u32[]{:S(2)}) %collective-permute-start.24) | collective-permute-done | bytes 360480 | tf_op jit(solution)/shard_map/ppermute | solution.py:231
  93.9 4.8 %collective-permute-done.17.mid_o.refs_3_ = bf16[352,512]{1,0:T(8,128)(2,1)S(1)} collective-permute-done((bf16[352,512]{1,0:T(8,128)(2,1)S(1)}, bf16[352,512]{1,0:T(8,128)(2,1)S(1)}, u32[]{:S(2)}, u32[]{:S(2)}) %collective-permute-start.17) | collective-permute-done | bytes 360480 | tf_op jit(solution)/shard_map/ppermute | solution.py:221
  98.7 7.7 %collective-permute-done.19.far_o.refs_5_ = bf16[352,512]{1,0:T(8,128)(2,1)S(1)} collective-permute-done((bf16[352,512]{1,0:T(8,128)(2,1)S(1)}, bf16[352,512]{1,0:T(8,128)(2,1)S(1)}, u32[]{:S(2)}, u32[]{:S(2)}) %collective-permute-start.19) | collective-permute-done | bytes 360480 | tf_op jit(solution)/shard_map/ppermute | solution.py:227
  109.3 4.7 %collective-permute-done.14.got = bf16[352,512]{1,0:T(8,128)(2,1)S(1)} collective-permute-done((bf16[352,512]{1,0:T(8,128)(2,1)S(1)}, bf16[352,512]{1,0:T(8,128)(2,1)S(1)}, u32[]{:S(2)}, u32[]{:S(2)}) %collective-permute-start.14) | collective-permute-done | bytes 360480 | tf_op jit(solution)/shard_map/ppermute | solution.py:253
  114.0 2.5 %shard_map.80 = (bf16[2,2,128,1024]{3,2,1,0:T(8,128)(2,1)S(1)}, bf16[2,2,128,1024]{3,2,1,0:T(8,128)(2,1)S(1)}) custom-call(bf16[4,512,512]{2,1,0:T(8,128)(2,1)S(1)} %get-tuple-element.15.gs, bf16[352,512]{1,0:T(8,128)(2,1)S(1)} %constant_dynamic-slice_fusion.refs_8_.d0, bf16[352,512]{1,0:T(8,128)(2,1)S(1)} %collective-permute-done.4.refs_9_.d1, ...), custom_call_target="tpu_custom_call" | custom-call | flops 2214592512 | bytes 9666560 | tf_op jit(solution)/shard_map/pallas_call | solution.py:79
  118.4 12.2 %collective-permute-start.37 = (bf16[176,512]{1,0:T(8,128)(2,1)S(1)}, bf16[176,512]{1,0:T(8,128)(2,1)S(1)}, u32[]{:S(2)}, u32[]{:S(2)}) collective-permute-start(bf16[176,512]{1,0:T(8,128)(2,1)S(1)} %fusion.11), channel_id=1, source_target_pairs={{0,4},{4,0},{8,12},{12,8},{1,5},{5,1},{9,13},{13,9},{2,6},{6,2},{1... | collective-permute-start | bytes 540680 | tf_op jit(solution)/shard_map/ppermute | solution.py:268
  130.7 7.1 %collective-permute-start.34 = (bf16[176,512]{1,0:T(8,128)(2,1)S(1)}, bf16[176,512]{1,0:T(8,128)(2,1)S(1)}, u32[]{:S(2)}, u32[]{:S(2)}) collective-permute-start(bf16[176,512]{1,0:T(8,128)(2,1)S(1)} %fusion.10), channel_id=1, source_target_pairs={{0,4},{4,0},{8,12},{12,8},{1,5},{5,1},{9,13},{13,9},{2,6},{6,2},{1... | collective-permute-start | bytes 540680 | tf_op jit(solution)/shard_map/ppermute | solution.py:268
  142.4 1.8 %collective-permute-start.40 = (f32[1,352]{1,0:T(1,128)S(1)}, f32[1,352]{1,0:T(1,128)S(1)}, u32[]{:S(2)}, u32[]{:S(2)}) collective-permute-start(f32[1,352]{1,0:T(1,128)S(1)} %reshape_broadcast_in_dim.3), channel_id=1, source_target_pairs={{0,4},{4,0},{8,12},{12,8},{1,5},{5,1},{9,13},{13,9},{2,6},{6,2},{1... | collective-permute-start | bytes 4232 | tf_op jit(solution)/shard_map/ppermute | solution.py:277
  144.2 1.8 %collective-permute-done.40 = f32[1,352]{1,0:T(1,128)S(1)} collective-permute-done((f32[1,352]{1,0:T(1,128)S(1)}, f32[1,352]{1,0:T(1,128)S(1)}, u32[]{:S(2)}, u32[]{:S(2)}) %collective-permute-start.40) | collective-permute-done | bytes 1440 | tf_op jit(solution)/shard_map/ppermute | solution.py:277
  146.0 2.5 %collective-permute-start.41 = (f32[1,352]{1,0:T(1,128)S(1)}, f32[1,352]{1,0:T(1,128)S(1)}, u32[]{:S(2)}, u32[]{:S(2)}) collective-permute-start(f32[1,352]{1,0:T(1,128)S(1)} %reshape_add_fusion), channel_id=1, source_target_pairs={{0,12},{12,0},{4,8},{8,4},{1,13},{13,1},{5,9},{9,5},{2,14},{14,2},... | collective-permute-start | bytes 4232 | tf_op jit(solution)/shard_map/ppermute | solution.py:278
  154.9 4.4 %collective-permute-done.42 = f32[1,352]{1,0:T(1,128)S(1)} collective-permute-done((f32[1,352]{1,0:T(1,128)S(1)}, f32[1,352]{1,0:T(1,128)S(1)}, u32[]{:S(2)}, u32[]{:S(2)}) %collective-permute-start.42) | collective-permute-done | bytes 1440 | tf_op jit(solution)/shard_map/ppermute | solution.py:279
  161.8 5.0 %collective-permute-done.27 = bf16[128,1024]{1,0:T(8,128)(2,1)S(1)} collective-permute-done((bf16[128,1024]{1,0:T(8,128)(2,1)S(1)}, bf16[128,1024]{1,0:T(8,128)(2,1)S(1)}, u32[]{:S(2)}, u32[]{:S(2)}) %collective-permute-start.27) | collective-permute-done | bytes 262176 | tf_op jit(solution)/shard_map/ppermute | solution.py:286
  (113 shorter events, 40.4 us)
Async XLA Ops:
  2.8 24.0 %collective-permute-start.20 = (bf16[352,512]{1,0:T(8,128)(2,1)S(1)}, bf16[352,512]{1,0:T(8,128)(2,1)S(1)}, u32[]{:S(2)}, u32[]{:S(2)}) collective-permute-start(bf16[352,512]{1,0:T(8,128)(2,1)S(1)} %pad_maximum_fusion.3.own.refs_6_), channel_id=1, source_target_pairs={{0,4},{4,0},{8,12},{12,8},{1,5},{5,1},{9,13},{13,9},{2,6},{6,2},{1... | collective-permute-start | bytes 1081352 | tf_op jit(solution)/shard_map/ppermute | solution.py:214
  6.0 13.3 %collective-permute-start.7 = (bf16[64,2048]{1,0:T(8,128)(2,1)S(1)}, bf16[64,2048]{1,0:T(8,128)(2,1)S(1)}, u32[]{:S(2)}, u32[]{:S(2)}) collective-permute-start(bf16[64,2048]{1,0:T(8,128)(2,1)S(1)} %constant_dynamic-slice_fusion.1), channel_id=1, source_target_pairs={{0,4},{12,8},{1,5},{13,9},{2,6},{14,10},{3,7},{15,11},{16,20},{28,... | collective-permute-start | bytes 786440 | tf_op jit(solution)/shard_map/ppermute | solution.py:219
  8.2 23.1 %collective-permute-start = (bf16[2,64,2048]{2,1,0:T(8,128)(2,1)S(1)}, bf16[2,64,2048]{2,1,0:T(8,128)(2,1)S(1)}, u32[]{:S(2)}, u32[]{:S(2)}) collective-permute-start(bf16[2,64,2048]{2,1,0:T(8,128)(2,1)S(1)} %pad_maximum_fusion), channel_id=1, source_target_pairs={{0,16},{16,0},{1,17},{17,1},{2,18},{18,2},{3,19},{19,3},{4,20},{20... | collective-permute-start | bytes 1572872 | tf_op jit(solution)/shard_map/ppermute | solution.py:216
  20.8 12.1 %collective-permute-start.21 = (bf16[352,512]{1,0:T(8,128)(2,1)S(1)}, bf16[352,512]{1,0:T(8,128)(2,1)S(1)}, u32[]{:S(2)}, u32[]{:S(2)}) collective-permute-start(bf16[352,512]{1,0:T(8,128)(2,1)S(1)} %pad_maximum_fusion.3.own.refs_6_), channel_id=1, source_target_pairs={{4,8},{8,4},{5,9},{9,5},{6,10},{10,6},{7,11},{11,7},{20,24},{24,20... | collective-permute-start | bytes 1081352 | tf_op jit(solution)/shard_map/ppermute | solution.py:215
  21.5 14.1 %collective-permute-start.15 = (bf16[352,512]{1,0:T(8,128)(2,1)S(1)}, bf16[352,512]{1,0:T(8,128)(2,1)S(1)}, u32[]{:S(2)}, u32[]{:S(2)}) collective-permute-start(bf16[352,512]{1,0:T(8,128)(2,1)S(1)} %pad_maximum_fusion.2.own.refs_0_), channel_id=1, source_target_pairs={{0,4},{4,0},{8,12},{12,8},{1,5},{5,1},{9,13},{13,9},{2,6},{6,2},{1... | collective-permute-start | bytes 1081352 | tf_op jit(solution)/shard_map/ppermute | solution.py:212
  27.6 13.2 %collective-permute-start.4 = (bf16[352,512]{1,0:T(8,128)(2,1)S(1)}, bf16[352,512]{1,0:T(8,128)(2,1)S(1)}, u32[]{:S(2)}, u32[]{:S(2)}) collective-permute-start(bf16[352,512]{1,0:T(8,128)(2,1)S(1)} %constant_dynamic-slice_fusion.refs_8_.d0), channel_id=1, source_target_pairs={{0,4},{12,8},{1,5},{13,9},{2,6},{14,10},{3,7},{15,11},{16,20},{28,... | collective-permute-start | bytes 1081352 | tf_op jit(solution)/shard_map/ppermute | solution.py:217
  31.3 14.9 %collective-permute-start.1 = (bf16[2,64,2048]{2,1,0:T(8,128)(2,1)S(1)}, bf16[2,64,2048]{2,1,0:T(8,128)(2,1)S(1)}, u32[]{:S(2)}, u32[]{:S(2)}) collective-permute-start(bf16[2,64,2048]{2,1,0:T(8,128)(2,1)S(1)} %collective-permute-done.refs_0_), channel_id=1, source_target_pairs={{0,2},{2,0},{1,3},{3,1},{4,6},{6,4},{5,7},{7,5},{8,10},{10,8},{9,1... | collective-permute-start | bytes 1572872 | tf_op jit(solution)/shard_map/ppermute | solution.py:224
  32.8 21.4 %collective-permute-start.9 = (bf16[2,64,2048]{2,1,0:T(8,128)(2,1)S(1)}, bf16[2,64,2048]{2,1,0:T(8,128)(2,1)S(1)}, u32[]{:S(2)}, u32[]{:S(2)}) collective-permute-start(bf16[2,64,2048]{2,1,0:T(8,128)(2,1)S(1)} %pad_maximum_fusion.1), channel_id=1, source_target_pairs={{0,2},{2,0},{1,3},{3,1},{4,6},{6,4},{5,7},{7,5},{8,10},{10,8},{9,1... | collective-permute-start | bytes 1572872 | tf_op jit(solution)/shard_map/ppermute | solution.py:232
  40.8 13.5 %collective-permute-start.18 = (bf16[352,512]{1,0:T(8,128)(2,1)S(1)}, bf16[352,512]{1,0:T(8,128)(2,1)S(1)}, u32[]{:S(2)}, u32[]{:S(2)}) collective-permute-start(bf16[352,512]{1,0:T(8,128)(2,1)S(1)} %collective-permute-done.15.pair.refs_1_), channel_id=1, source_target_pairs={{4,8},{8,4},{5,9},{9,5},{6,10},{10,6},{7,11},{11,7},{20,24},{24,20... | collective-permute-start | bytes 1081352 | tf_op jit(solution)/shard_map/ppermute | solution.py:220
  42.3 12.6 %collective-permute-start.6 = (bf16[352,512]{1,0:T(8,128)(2,1)S(1)}, bf16[352,512]{1,0:T(8,128)(2,1)S(1)}, u32[]{:S(2)}, u32[]{:S(2)}) collective-permute-start(bf16[352,512]{1,0:T(8,128)(2,1)S(1)} %collective-permute-done.4.refs_9_.d1), channel_id=1, source_target_pairs={{4,8},{8,4},{5,9},{9,5},{6,10},{10,6},{7,11},{11,7},{20,24},{24,20... | collective-permute-start | bytes 1081352 | tf_op jit(solution)/shard_map/ppermute | solution.py:228
  43.0 13.3 %collective-permute-start.2 = (bf16[2,64,2048]{2,1,0:T(8,128)(2,1)S(1)}, bf16[2,64,2048]{2,1,0:T(8,128)(2,1)S(1)}, u32[]{:S(2)}, u32[]{:S(2)}) collective-permute-start(bf16[2,64,2048]{2,1,0:T(8,128)(2,1)S(1)} %collective-permute-done.refs_0_), channel_id=1, source_target_pairs={{0,1},{1,0},{2,3},{3,2},{4,5},{5,4},{6,7},{7,6},{8,9},{9,8},{10,11... | collective-permute-start | bytes 1572872 | tf_op jit(solution)/shard_map/ppermute | solution.py:226
  55.0 28.3 %collective-permute-start.22 = (bf16[352,512]{1,0:T(8,128)(2,1)S(1)}, bf16[352,512]{1,0:T(8,128)(2,1)S(1)}, u32[]{:S(2)}, u32[]{:S(2)}) collective-permute-start(bf16[352,512]{1,0:T(8,128)(2,1)S(1)} %collective-permute-done.21.mid_i.refs_8_), channel_id=1, source_target_pairs={{4,0},{8,12},{5,1},{9,13},{6,2},{10,14},{7,3},{11,15},{20,16},{24,... | collective-permute-start | bytes 1081352 | tf_op jit(solution)/shard_map/ppermute | solution.py:223
  56.3 34.7 %collective-permute-start.24 = (bf16[352,512]{1,0:T(8,128)(2,1)S(1)}, bf16[352,512]{1,0:T(8,128)(2,1)S(1)}, u32[]{:S(2)}, u32[]{:S(2)}) collective-permute-start(bf16[352,512]{1,0:T(8,128)(2,1)S(1)} %collective-permute-done.23.far_i.refs_10_), channel_id=1, source_target_pairs={{4,0},{8,12},{5,1},{9,13},{6,2},{10,14},{7,3},{11,15},{20,16},{24,... | collective-permute-start | bytes 1081352 | tf_op jit(solution)/shard_map/ppermute | solution.py:231
  57.6 41.1 %collective-permute-start.17 = (bf16[352,512]{1,0:T(8,128)(2,1)S(1)}, bf16[352,512]{1,0:T(8,128)(2,1)S(1)}, u32[]{:S(2)}, u32[]{:S(2)}) collective-permute-start(bf16[352,512]{1,0:T(8,128)(2,1)S(1)} %collective-permute-done.16.mid_i.refs_2_), channel_id=1, source_target_pairs={{4,0},{8,12},{5,1},{9,13},{6,2},{10,14},{7,3},{11,15},{20,16},{24,... | collective-permute-start | bytes 1081352 | tf_op jit(solution)/shard_map/ppermute | solution.py:221
  58.9 47.5 %collective-permute-start.19 = (bf16[352,512]{1,0:T(8,128)(2,1)S(1)}, bf16[352,512]{1,0:T(8,128)(2,1)S(1)}, u32[]{:S(2)}, u32[]{:S(2)}) collective-permute-start(bf16[352,512]{1,0:T(8,128)(2,1)S(1)} %collective-permute-done.18.far_i.refs_4_), channel_id=1, source_target_pairs={{4,0},{8,12},{5,1},{9,13},{6,2},{10,14},{7,3},{11,15},{20,16},{24,... | collective-permute-start | bytes 1081352 | tf_op jit(solution)/shard_map/ppermute | solution.py:227
  60.3 53.7 %collective-permute-start.14 = (bf16[352,512]{1,0:T(8,128)(2,1)S(1)}, bf16[352,512]{1,0:T(8,128)(2,1)S(1)}, u32[]{:S(2)}, u32[]{:S(2)}) collective-permute-start(bf16[352,512]{1,0:T(8,128)(2,1)S(1)} %shard_map.77), channel_id=1, source_target_pairs={{4,0},{8,12},{5,1},{9,13},{6,2},{10,14},{7,3},{11,15},{20,16},{24,... | collective-permute-start | bytes 1081352 | tf_op jit(solution)/shard_map/ppermute | solution.py:253
  92.4 24.2 %collective-permute-start.35 = (bf16[2,176,512]{2,1,0:T(8,128)(2,1)S(1)}, bf16[2,176,512]{2,1,0:T(8,128)(2,1)S(1)}, u32[]{:S(2)}, u32[]{:S(2)}) collective-permute-start(bf16[2,176,512]{2,1,0:T(8,128)(2,1)S(1)} %get-tuple-element.26), channel_id=1, source_target_pairs={{0,4},{12,8},{1,5},{13,9},{2,6},{14,10},{3,7},{15,11},{16,20},{28,... | collective-permute-start | bytes 1081352 | tf_op jit(solution)/shard_map/ppermute | solution.py:246
  116.5 21.4 %collective-permute-start.25 = (bf16[2,2,128,1024]{3,2,1,0:T(8,128)(2,1)S(1)}, bf16[2,2,128,1024]{3,2,1,0:T(8,128)(2,1)S(1)}, u32[]{:S(2)}, u32[]{:S(2)}) collective-permute-start(bf16[2,2,128,1024]{3,2,1,0:T(8,128)(2,1)S(1)} %get-tuple-element.20), channel_id=1, source_target_pairs={{0,1},{1,0},{2,3},{3,2},{4,5},{5,4},{6,7},{7,6},{8,9},{9,8},{10,11... | collective-permute-start | bytes 3145736 | tf_op jit(solution)/shard_map/ppermute | solution.py:262
  117.5 13.0 %collective-permute-start.33 = (bf16[2,176,512]{2,1,0:T(8,128)(2,1)S(1)}, bf16[2,176,512]{2,1,0:T(8,128)(2,1)S(1)}, u32[]{:S(2)}, u32[]{:S(2)}) collective-permute-start(bf16[2,176,512]{2,1,0:T(8,128)(2,1)S(1)} %add_convert_fusion.2), channel_id=1, source_target_pairs={{4,8},{8,4},{5,9},{9,5},{6,10},{10,6},{7,11},{11,7},{20,24},{24,20... | collective-permute-start | bytes 1081352 | tf_op jit(solution)/shard_map/ppermute | solution.py:255
  118.4 19.4 %collective-permute-start.37 = (bf16[176,512]{1,0:T(8,128)(2,1)S(1)}, bf16[176,512]{1,0:T(8,128)(2,1)S(1)}, u32[]{:S(2)}, u32[]{:S(2)}) collective-permute-start(bf16[176,512]{1,0:T(8,128)(2,1)S(1)} %fusion.11), channel_id=1, source_target_pairs={{0,4},{4,0},{8,12},{12,8},{1,5},{5,1},{9,13},{13,9},{2,6},{6,2},{1... | collective-permute-start | bytes 540680 | tf_op jit(solution)/shard_map/ppermute | solution.py:268
  130.7 11.4 %collective-permute-start.34 = (bf16[176,512]{1,0:T(8,128)(2,1)S(1)}, bf16[176,512]{1,0:T(8,128)(2,1)S(1)}, u32[]{:S(2)}, u32[]{:S(2)}) collective-permute-start(bf16[176,512]{1,0:T(8,128)(2,1)S(1)} %fusion.10), channel_id=1, source_target_pairs={{0,4},{4,0},{8,12},{12,8},{1,5},{5,1},{9,13},{13,9},{2,6},{6,2},{1... | collective-permute-start | bytes 540680 | tf_op jit(solution)/shard_map/ppermute | solution.py:268
  138.3 13.6 %collective-permute-start.26 = (bf16[128,1024]{1,0:T(8,128)(2,1)S(1)}, bf16[128,1024]{1,0:T(8,128)(2,1)S(1)}, u32[]{:S(2)}, u32[]{:S(2)}) collective-permute-start(bf16[128,1024]{1,0:T(8,128)(2,1)S(1)} %get-tuple-element.30), channel_id=1, source_target_pairs={{0,16},{16,0},{1,17},{17,1},{2,18},{18,2},{3,19},{19,3},{4,20},{20... | collective-permute-start | bytes 786440 | tf_op jit(solution)/shard_map/ppermute | solution.py:284
  138.9 14.3 %collective-permute-start.28 = (bf16[128,1024]{1,0:T(8,128)(2,1)S(1)}, bf16[128,1024]{1,0:T(8,128)(2,1)S(1)}, u32[]{:S(2)}, u32[]{:S(2)}) collective-permute-start(bf16[128,1024]{1,0:T(8,128)(2,1)S(1)} %get-tuple-element.29), channel_id=1, source_target_pairs={{0,16},{16,0},{1,17},{17,1},{2,18},{18,2},{3,19},{19,3},{4,20},{20... | collective-permute-start | bytes 786440 | tf_op jit(solution)/shard_map/ppermute | solution.py:284
  148.5 11.6 %collective-permute-start.39 = (bf16[176,512]{1,0:T(8,128)(2,1)S(1)}, bf16[176,512]{1,0:T(8,128)(2,1)S(1)}, u32[]{:S(2)}, u32[]{:S(2)}) collective-permute-start(bf16[176,512]{1,0:T(8,128)(2,1)S(1)} %fusion.5), channel_id=1, source_target_pairs={{0,16},{16,0},{1,17},{17,1},{2,18},{18,2},{3,19},{19,3},{4,20},{20... | collective-permute-start | bytes 540680 | tf_op jit(solution)/shard_map/ppermute | solution.py:270
  (24 other events, 185.6 us)

commit v2 on v1

--- a/solution.py
+++ b/solution.py
@@ -1,3 +1,5 @@
+import functools
+
 import jax
 import jax.numpy as jnp
 from jax import lax
@@ -52,6 +54,8 @@
 OVER_X = ((0, 2), (2, 0), (1, 3), (3, 1))
 OVER_CORE = ((0, 1), (1, 0), (2, 3), (3, 2))
 
+FIRST_CHUNK = 8
+
 
 def paired(tokens, gate_weight, up_weight, down_weight, out_grad):
     return paired_body(tokens, gate_weight, up_weight, down_weight, out_grad)
@@ -74,7 +78,7 @@
 
 
 def call(kernel, outs, scratch=(), flops=0, limit=28):
-    def run(*args):
+    def inner_call(*args):
         size = sum(v.size * v.dtype.itemsize for v in args)
         return pl.pallas_call(
             kernel,
@@ -86,7 +90,7 @@
             cost_estimate=pl.CostEstimate(flops=flops, bytes_accessed=size, transcendentals=0),
         )(*args)
 
-    return run
+    return inner_call
 
 
 def like(shape, dtype):
@@ -135,37 +139,45 @@
 
 
 def pair_kernel(*refs):
-    parts, ws, (out,), (cols,) = refs[:8], refs[8:12], refs[12:13], refs[13:]
-    quarter, depth = parts[0].shape[0], cols.shape[2]
+    groups, ws, (out,), (cols,) = refs[:4], refs[4:8], refs[8:9], refs[9:]
+    quarter, depth = groups[0].shape[0], cols.shape[2]
 
     @pl.when(is_inner())
     def _():
         for p, place in enumerate(line_places()):
             at = pl.ds(pl.multiple_of(place * depth, depth), depth)
-            for i in range(8):
-                cols[p, pl.ds(i * quarter, quarter), :] = parts[i][:, at]
+            for i in range(4):
+                cols[p, pl.ds(i * quarter, quarter), :] = groups[i][:, at]
         out[...] = project([w[...] for w in ws], cols).astype(BF16)
 
 
-def back_kernel(gs, d0, d1, d2, d3, got, pre_a, pre_b, *refs):
+def own_kernel(gs, d0, d1, d2, d3, out):
+    @pl.when(is_inner())
+    def _():
+        out[...] = project((d0[...], d1[...], d2[...], d3[...]), gs)
+
+
+def back_kernel(group, parts, hid_own, got, pre_a, pre_b, *refs):
     weights, (keep, give), (hid,) = (refs[:6], refs[6:12]), refs[12:14], refs[14:]
     inner = is_inner()
-    half, count = hid.shape
-    part, rows = half // 2, count // 4
+    count = hid.shape[1]
+    tok = slice(group * count, (group + 1) * count)
 
     @pl.when(inner)
     def _():
-        hid[...] = project((d0[...], d1[...], d2[...], d3[...]), gs)
+        hid[...] = hid_own[:, tok]
 
     @pl.when(jnp.logical_not(inner))
     def _():
         hid[...] = got[...].astype(F32)
 
     grads = []
-    for c, pre in enumerate((pre_a, pre_b)):
-        _, gate_grad, up_grad = pointwise(pre[:part, :], pre[part:, :], hid[c * part:(c + 1) * part, :])
+    begin = 0
+    for part, pre in zip(parts, (pre_a, pre_b)):
+        _, gate_grad, up_grad = pointwise(pre[:part, tok], pre[part:, tok], hid[begin:begin + part, :])
+        begin += part
         grads.append(jnp.concatenate([gate_grad, up_grad], 0))
-    width = keep.shape[-1]
+    rows, depth = keep.shape[1], keep.shape[2] // 2
     for p in range(4):
         total = None
         for c in range(2):
@@ -174,11 +186,29 @@
             term = contract_first(grads[c], w)
             total = term if total is None else total + term
         total = total.astype(BF16)
-        at = pl.ds((p % 2) * (width // 2), width // 2)
-        for group in range(2):
-            base = group * 2 * rows
-            keep[p // 2, group, :, at] = total[base:base + rows]
-            give[p // 2, group, :, at] = total[base + rows:base + 2 * rows]
+        at = pl.ds((p % 2) * depth, depth)
+        keep[p // 2, :, at] = total[:rows]
+        give[p // 2, :, at] = total[rows:]
+
+
+def near_kernel(near, got, owned, paired_sum):
+    owned[...] = near[0] + got[0].astype(F32)
+    paired_sum[...] = (near[1] + got[1].astype(F32)).astype(BF16)
+
+
+def add_kernel(a, b, out):
+    out[...] = (a[...].astype(F32) + b[...].astype(F32)).astype(out.dtype)
+
+
+def add_halves_kernel(a, b, *outs):
+    for i, out in enumerate(outs):
+        out[...] = (a[i].astype(F32) + b[i].astype(F32)).astype(BF16)
+
+
+def add_flipped_kernel(a, b, out):
+    half = a.shape[0] // 2
+    out[:half] = (a[:half].astype(F32) + b[half:].astype(F32)).astype(BF16)
+    out[half:] = (a[half:].astype(F32) + b[:half].astype(F32)).astype(BF16)
 
 
 def place_kernel(*refs):
@@ -199,10 +229,12 @@
     rows, width = tokens.shape
     units, depth = down_weight.shape
     half, quarter = units // 2, rows // 4
-    part, count = half // 2, 2 * rows
+    count = 2 * rows
+    long = half * FIRST_CHUNK // 16 // 16 * 16
+    parts, begins = (long, half - long), (0, long)
 
     def my_part(w, c):
-        return lax.dynamic_slice_in_dim(w, y * half + c * part, part, 0)
+        return lax.dynamic_slice_in_dim(w, y * half + begins[c], parts[c], 0)
 
     gate_t, up_t = gate_weight.T, up_weight.T
     gu = [jnp.concatenate([my_part(gate_t, c), my_part(up_t, c)], 0) for c in range(2)]
@@ -239,34 +271,41 @@
     gu_sets = ((gu[0], p1a, p2a, p4a, p3a, p5a), (gu[1], p1b, p2b, p4b, p3b, p5b))
     fronts = []
     for c in range(2):
-        outs = [like((half, count), F32)] + [like((2, part, depth), d) for d in (F32, F32, BF16)]
-        fronts.append(call(front_kernel, outs, flops=2 * count * width * (half + part))(xs, gs, *gu_sets[c]))
+        outs = [like((2 * parts[c], count), F32)] + [like((2, parts[c], depth), d) for d in (F32, F32, BF16)]
+        fronts.append(call(front_kernel, outs, flops=6 * count * width * parts[c])(xs, gs, *gu_sets[c]))
     gots = []
     for c in range(2):
         got = lax.ppermute(fronts[c][3], "fs", INWARD)
-        gots.append((fronts[c][2] + got.astype(F32)).astype(BF16))
+        far = fronts[c][2]
+        gots += call(add_kernel, [like(far.shape, BF16)])(far, got)
 
     down_pieces = (down_h, p1d, p2d, p3d)
-    (pair_hid,) = call(
-        pair_kernel, [like((half, count), BF16)], [pltpu.VMEM((4, count, depth), BF16)], flops=2 * count * width * half
-    )(*gp, *down_pieces)
-    hid_got = lax.ppermute(pair_hid, "fs", OUTWARD)
-
-    gots = [lax.ppermute(gots[c], "fs", MIDDLE).astype(F32) for c in range(2)]
-    keep, give = call(
-        back_kernel,
-        [like((2, 2, rows // 2, width // 2), BF16)] * 2,
-        [pltpu.VMEM((half, count), F32)],
-        flops=6 * count * width * half,
-    )(gs, *down_pieces, hid_got, fronts[0][0], fronts[1][0], *gu_sets[0], *gu_sets[1])
-    got = lax.ppermute(give, "tp", OVER_CORE)
-    halved = (keep.astype(F32) + got.astype(F32)).astype(BF16)
+    hid_gots = [None, None]
+    for group in (1, 0):
+        (pair_hid,) = call(
+            pair_kernel, [like((half, rows), BF16)], [pltpu.VMEM((4, rows, depth), BF16)], flops=2 * rows * width * half
+        )(*gp[4 * group:4 * group + 4], *down_pieces)
+        hid_gots[group] = lax.ppermute(pair_hid, "fs", OUTWARD)
+    (own_hid,) = call(own_kernel, [like((half, count), F32)], flops=2 * count * width * half)(gs, *down_pieces)
+
+    gots = [lax.ppermute(gots[c], "fs", MIDDLE) for c in range(2)]
+    halves = [None, None]
+    for group in (1, 0):
+        keep, give = call(
+            functools.partial(back_kernel, group, parts),
+            [like((2, rows // 2, width // 2), BF16)] * 2,
+            [pltpu.VMEM((half, rows), F32)],
+            flops=4 * rows * width * half,
+        )(own_hid, hid_gots[group], fronts[0][0], fronts[1][0], *gu_sets[0], *gu_sets[1])
+        got = lax.ppermute(give, "tp", OVER_CORE)
+        halves[group] = call(add_halves_kernel, [like(keep.shape[1:], BF16)] * 2)(keep, got)
 
     finals = []
     for c in range(2):
-        near = fronts[c][1]
-        last = lax.ppermute((near[1] + gots[c][1]).astype(BF16), "fs", OUTER_PAIRS).astype(F32)
-        finals.append((near[0] + gots[c][0] + last).astype(BF16))
+        block = gots[c].shape[1:]
+        owned, paired_sum = call(near_kernel, [like(block, F32), like(block, BF16)])(fronts[c][1], gots[c])
+        last = lax.ppermute(paired_sum, "fs", OUTER_PAIRS)
+        finals += call(add_kernel, [like(block, BF16)])(owned, last)
     peers = [lax.ppermute(finals[c], "rep", SWAP) for c in range(2)]
     final_own, peers = jnp.concatenate(finals, 0), jnp.concatenate(peers, 0)
     low = jnp.where(y == 0, final_own, peers)
@@ -281,11 +320,10 @@
 
     done = []
     for i in range(2):
-        got = lax.ppermute(halved[i, 1], "rep", SWAP)
-        mine = (halved[i, 0].astype(F32) + got.astype(F32)).astype(BF16)
+        got = lax.ppermute(halves[1][i], "rep", SWAP)
+        (mine,) = call(add_kernel, [like(got.shape, BF16)])(halves[0][i], got)
         got = lax.ppermute(mine, "tp", OVER_X)
-        flipped = jnp.concatenate([got[quarter:], got[:quarter]], 0)
-        done.append((mine.astype(F32) + flipped.astype(F32)).astype(BF16))
+        done += call(add_flipped_kernel, [like(got.shape, BF16)])(mine, got)
     done += [lax.ppermute(done[i], "tp", OVER_CORE) for i in range(2)]
     (input_grad,) = call(place_kernel, [like((rows, width), BF16)])(*done)
     return input_grad, down_grad, norms

time: 170 us -> 158 us (0.929)
  waiting for transfers between devices: 88.5 us -> 80.4 us
  starting transfers between devices: 67 us -> 61 us
  local copies, waits for them, and re-layouts: 2.39 us -> 4.21 us
    ppermute x1, waiting for transfers between devices: 9.03 us -> 1.93 us  [paired_body(): gp[0] = lax.ppermute(mine[1], 'fs', INWARD)]
    ppermute x1, waiting for transfers between devices: 0.01 us -> 6.78 us  [paired_body(): gp[4] = lax.ppermute(gp[0], 'rep', SWAP)]
    ppermute x7 -> x8, starting transfers between devices: 24 us -> 17.7 us  [the longest x2 11.7 us: paired_body(): last = lax.ppermute(paired_sum, 'fs', OUTER_PAIRS)]
    ppermute x2, waiting for transfers between devices: 5 us -> 0.02 us  [paired_body(): got = lax.ppermute(mine, 'tp', OVER_X)]
    ppermute x1, waiting for transfers between devices: 4.41 us -> 0.05 us  [paired_body(): norm_peer = lax.ppermute(norm, 'rep', SWAP)]
    ppermute x2, waiting for transfers between devices: 0.01 us -> 3.89 us  [paired_body(): peers = [lax.ppermute(finals[c], 'rep', SWAP) for c in range(2)]]
    ppermute x1, starting transfers between devices: 2.11 us -> 4.97 us  [paired_body(): gp[0] = lax.ppermute(mine[1], 'fs', INWARD)]
    ppermute x1, waiting for transfers between devices: 0.87 us -> 3.34 us  [paired_body(): norm = norm + lax.ppermute(norm, 'fs', ACROSS)]
  transfers between devices with their start and end apart: 43 -> 45, of which waited for: 18 -> 14; matrix products, arithmetic and copies ran while one was open for 2% -> 4% of each run, Pallas kernels for 3% -> 4%
where the time goes in v2:
time: 158 us; the launch traced here: 157 us
  waiting for transfers between devices  80.4 us (51%)
  starting transfers between devices  61 us (39%)
  Pallas kernels  7.79 us (5%)
  local copies, waits for them, and re-layouts  4.21 us (3%)
  other arithmetic  2.43 us (2%)
    ppermute x1, waiting for transfers between devices, paired_body(): p4b = lax.ppermute(p2b, 'fs', OUTWARD)  21.2 us
    ppermute x2, starting transfers between devices, paired_body(): last = lax.ppermute(paired_sum, 'fs', OUTER_PAIRS)  11.7 us
    ppermute x1, waiting for transfers between devices, paired_body(): gp_x = lax.ppermute(jnp.stack([gp[0], gp[4]], 0), 'tp', OVER_X)  8.97 us
    pallas_call x21, Pallas kernels, inner_call(): pl.pallas_call(kernel, out_shape=outs, in_specs=[pl.BlockSpec(memory_spac...  7.79 us
    ppermute x1, waiting for transfers between devices, paired_body(): p5b = lax.ppermute(p3b, 'fs', OUTWARD)  7.72 us
    ppermute x1, waiting for transfers between devices, paired_body(): gp[4] = lax.ppermute(gp[0], 'rep', SWAP)  6.78 us
    ppermute x1, waiting for transfers between devices, paired_body(): p5a = lax.ppermute(p3a, 'fs', OUTWARD)  6.06 us
    ppermute x1, waiting for transfers between devices, paired_body(): p4a = lax.ppermute(p2a, 'fs', OUTWARD)  5.02 us
  transfers between devices with their start and end apart: 45, of which 14 were waited for; matrix products, arithmetic and copies ran while one was open for 4% of the time, Pallas kernels for 4%

profile of v2, /device:TPU:0, one launch (start us, length us, event | category | flops | bytes accessed | tf_op | source)
XLA Modules:
  0.0 157.1 jit_solution(4003872172138152129)
XLA Ops:
  1.7 5.0 %collective-permute-start.7 = (bf16[64,2048]{1,0:T(8,128)(2,1)S(1)}, bf16[64,2048]{1,0:T(8,128)(2,1)S(1)}, u32[]{:S(2)}, u32[]{:S(2)}) collective-permute-start(bf16[64,2048]{1,0:T(8,128)(2,1)S(1)} %constant_dynamic-slice_fusion.1), channel_id=1, source_target_pairs={{0,4},{12,8},{1,5},{13,9},{2,6},{14,10},{3,7},{15,11},{16,20},{28,... | collective-permute-start | bytes 786440 | tf_op jit(solution)/shard_map/ppermute | solution.py:251
  8.7 1.6 %collective-permute-start = (bf16[2,64,2048]{2,1,0:T(8,128)(2,1)S(1)}, bf16[2,64,2048]{2,1,0:T(8,128)(2,1)S(1)}, u32[]{:S(2)}, u32[]{:S(2)}) collective-permute-start(bf16[2,64,2048]{2,1,0:T(8,128)(2,1)S(1)} %pad_maximum_fusion), channel_id=1, source_target_pairs={{0,16},{16,0},{1,17},{17,1},{2,18},{18,2},{3,19},{19,3},{4,20},{20... | collective-permute-start | bytes 1572872 | tf_op jit(solution)/shard_map/ppermute | solution.py:248
  10.3 1.9 %collective-permute-done.7.refs_0_ = bf16[64,2048]{1,0:T(8,128)(2,1)S(1)} collective-permute-done((bf16[64,2048]{1,0:T(8,128)(2,1)S(1)}, bf16[64,2048]{1,0:T(8,128)(2,1)S(1)}, u32[]{:S(2)}, u32[]{:S(2)}) %collective-permute-start.7) | collective-permute-done | bytes 262176 | tf_op jit(solution)/shard_map/ppermute | solution.py:251
  14.9 2.5 %collective-permute-start.18 = (bf16[352,512]{1,0:T(8,128)(2,1)S(1)}, bf16[352,512]{1,0:T(8,128)(2,1)S(1)}, u32[]{:S(2)}, u32[]{:S(2)}) collective-permute-start(bf16[352,512]{1,0:T(8,128)(2,1)S(1)} %pad_maximum_fusion.3.own.refs_6_), channel_id=1, source_target_pairs={{0,4},{4,0},{8,12},{12,8},{1,5},{5,1},{9,13},{13,9},{2,6},{6,2},{1... | collective-permute-start | bytes 1081352 | tf_op jit(solution)/shard_map/ppermute | solution.py:246
  18.1 2.9 %collective-permute-start.13 = (bf16[352,512]{1,0:T(8,128)(2,1)S(1)}, bf16[352,512]{1,0:T(8,128)(2,1)S(1)}, u32[]{:S(2)}, u32[]{:S(2)}) collective-permute-start(bf16[352,512]{1,0:T(8,128)(2,1)S(1)} %pad_maximum_fusion.2.own.refs_0_), channel_id=1, source_target_pairs={{0,4},{4,0},{8,12},{12,8},{1,5},{5,1},{9,13},{13,9},{2,6},{6,2},{1... | collective-permute-start | bytes 1081352 | tf_op jit(solution)/shard_map/ppermute | solution.py:244
  21.0 6.8 %collective-permute-done.8.refs_0_ = bf16[64,2048]{1,0:T(8,128)(2,1)S(1)} collective-permute-done((bf16[64,2048]{1,0:T(8,128)(2,1)S(1)}, bf16[64,2048]{1,0:T(8,128)(2,1)S(1)}, u32[]{:S(2)}, u32[]{:S(2)}) %collective-permute-start.8) | collective-permute-done | bytes 262176 | tf_op jit(solution)/shard_map/ppermute | solution.py:262
  28.6 1.6 collective-permute-start.1
  30.7 4.4 %collective-permute-start.4 = (bf16[352,512]{1,0:T(8,128)(2,1)S(1)}, bf16[352,512]{1,0:T(8,128)(2,1)S(1)}, u32[]{:S(2)}, u32[]{:S(2)}) collective-permute-start(bf16[352,512]{1,0:T(8,128)(2,1)S(1)} %constant_dynamic-slice_fusion.d0.refs_4_), channel_id=1, source_target_pairs={{0,4},{12,8},{1,5},{13,9},{2,6},{14,10},{3,7},{15,11},{16,20},{28,... | collective-permute-start | bytes 1081352 | tf_op jit(solution)/shard_map/ppermute | solution.py:249
  36.5 4.5 %collective-permute-done.4.d1.refs_5_ = bf16[352,512]{1,0:T(8,128)(2,1)S(1)} collective-permute-done((bf16[352,512]{1,0:T(8,128)(2,1)S(1)}, bf16[352,512]{1,0:T(8,128)(2,1)S(1)}, u32[]{:S(2)}, u32[]{:S(2)}) %collective-permute-start.4) | collective-permute-done | bytes 360480 | tf_op jit(solution)/shard_map/ppermute | solution.py:249
  43.4 9.0 %collective-permute-done.9 = bf16[2,64,2048]{2,1,0:T(8,128)(2,1)S(1)} collective-permute-done((bf16[2,64,2048]{2,1,0:T(8,128)(2,1)S(1)}, bf16[2,64,2048]{2,1,0:T(8,128)(2,1)S(1)}, u32[]{:S(2)}, u32[]{:S(2)}) %collective-permute-start.9) | collective-permute-done | bytes 524320 | tf_op jit(solution)/shard_map/ppermute | solution.py:264
  58.9 21.2 %collective-permute-done.20.mid_o.refs_9_ = bf16[352,512]{1,0:T(8,128)(2,1)S(1)} collective-permute-done((bf16[352,512]{1,0:T(8,128)(2,1)S(1)}, bf16[352,512]{1,0:T(8,128)(2,1)S(1)}, u32[]{:S(2)}, u32[]{:S(2)}) %collective-permute-start.20) | collective-permute-done | bytes 360480 | tf_op jit(solution)/shard_map/ppermute | solution.py:255
  80.1 7.7 %collective-permute-done.22.far_o.refs_11_ = bf16[352,512]{1,0:T(8,128)(2,1)S(1)} collective-permute-done((bf16[352,512]{1,0:T(8,128)(2,1)S(1)}, bf16[352,512]{1,0:T(8,128)(2,1)S(1)}, u32[]{:S(2)}, u32[]{:S(2)}) %collective-permute-start.22) | collective-permute-done | bytes 360480 | tf_op jit(solution)/shard_map/ppermute | solution.py:263
  90.5 5.0 %collective-permute-done.15.mid_o.refs_3_ = bf16[352,512]{1,0:T(8,128)(2,1)S(1)} collective-permute-done((bf16[352,512]{1,0:T(8,128)(2,1)S(1)}, bf16[352,512]{1,0:T(8,128)(2,1)S(1)}, u32[]{:S(2)}, u32[]{:S(2)}) %collective-permute-start.15) | collective-permute-done | bytes 360480 | tf_op jit(solution)/shard_map/ppermute | solution.py:253
  97.0 6.1 %collective-permute-done.17.far_o.refs_5_ = bf16[352,512]{1,0:T(8,128)(2,1)S(1)} collective-permute-done((bf16[352,512]{1,0:T(8,128)(2,1)S(1)}, bf16[352,512]{1,0:T(8,128)(2,1)S(1)}, u32[]{:S(2)}, u32[]{:S(2)}) %collective-permute-start.17) | collective-permute-done | bytes 360480 | tf_op jit(solution)/shard_map/ppermute | solution.py:259
  111.6 4.7 %collective-permute-done.12.got = bf16[352,256]{1,0:T(8,128)(2,1)S(1)} collective-permute-done((bf16[352,256]{1,0:T(8,128)(2,1)S(1)}, bf16[352,256]{1,0:T(8,128)(2,1)S(1)}, u32[]{:S(2)}, u32[]{:S(2)}) %collective-permute-start.12) | collective-permute-done | bytes 180256 | tf_op jit(solution)/shard_map/ppermute | solution.py:288
  117.8 1.6 %collective-permute-start.30 = (bf16[128,1024]{1,0:T(8,128)(2,1)S(1)}, bf16[128,1024]{1,0:T(8,128)(2,1)S(1)}, u32[]{:S(2)}, u32[]{:S(2)}) collective-permute-start(bf16[128,1024]{1,0:T(8,128)(2,1)S(1)} %get-tuple-element.36), channel_id=1, source_target_pairs={{0,16},{16,0},{1,17},{17,1},{2,18},{18,2},{3,19},{19,3},{4,20},{20... | collective-permute-start | bytes 786440 | tf_op jit(solution)/shard_map/ppermute | solution.py:323
  120.0 4.8 %collective-permute-start.39 = (bf16[176,512]{1,0:T(8,128)(2,1)S(1)}, bf16[176,512]{1,0:T(8,128)(2,1)S(1)}, u32[]{:S(2)}, u32[]{:S(2)}) collective-permute-start(bf16[176,512]{1,0:T(8,128)(2,1)S(1)} %get-tuple-element.46), channel_id=1, source_target_pairs={{0,4},{4,0},{8,12},{12,8},{1,5},{5,1},{9,13},{13,9},{2,6},{6,2},{1... | collective-permute-start | bytes 540680 | tf_op jit(solution)/shard_map/ppermute | solution.py:307
  124.9 6.9 %collective-permute-start.36 = (bf16[176,512]{1,0:T(8,128)(2,1)S(1)}, bf16[176,512]{1,0:T(8,128)(2,1)S(1)}, u32[]{:S(2)}, u32[]{:S(2)}) collective-permute-start(bf16[176,512]{1,0:T(8,128)(2,1)S(1)} %get-tuple-element.41), channel_id=1, source_target_pairs={{0,4},{4,0},{8,12},{12,8},{1,5},{5,1},{9,13},{13,9},{2,6},{6,2},{1... | collective-permute-start | bytes 540680 | tf_op jit(solution)/shard_map/ppermute | solution.py:307
  131.8 4.0 %collective-permute-done.36.b = bf16[176,512]{1,0:T(8,128)(2,1)S(1)} collective-permute-done((bf16[176,512]{1,0:T(8,128)(2,1)S(1)}, bf16[176,512]{1,0:T(8,128)(2,1)S(1)}, u32[]{:S(2)}, u32[]{:S(2)}) %collective-permute-start.36) | collective-permute-done | bytes 180256 | tf_op jit(solution)/shard_map/ppermute | solution.py:307
  136.0 1.8 %collective-permute-start.42 = (f32[1,352]{1,0:T(1,128)S(1)}, f32[1,352]{1,0:T(1,128)S(1)}, u32[]{:S(2)}, u32[]{:S(2)}) collective-permute-start(f32[1,352]{1,0:T(1,128)S(1)} %reshape_broadcast_in_dim.3), channel_id=1, source_target_pairs={{0,4},{4,0},{8,12},{12,8},{1,5},{5,1},{9,13},{13,9},{2,6},{6,2},{1... | collective-permute-start | bytes 4232 | tf_op jit(solution)/shard_map/ppermute | solution.py:316
  138.0 1.6 collective-permute-start.31
  140.2 2.0 %collective-permute-start.43 = (f32[1,352]{1,0:T(1,128)S(1)}, f32[1,352]{1,0:T(1,128)S(1)}, u32[]{:S(2)}, u32[]{:S(2)}) collective-permute-start(f32[1,352]{1,0:T(1,128)S(1)} %reshape_add_fusion), channel_id=1, source_target_pairs={{0,12},{12,0},{4,8},{8,4},{1,13},{13,1},{5,9},{9,5},{2,14},{14,2},... | collective-permute-start | bytes 4232 | tf_op jit(solution)/shard_map/ppermute | solution.py:317
  142.3 3.3 %collective-permute-done.43 = f32[1,352]{1,0:T(1,128)S(1)} collective-permute-done((f32[1,352]{1,0:T(1,128)S(1)}, f32[1,352]{1,0:T(1,128)S(1)}, u32[]{:S(2)}, u32[]{:S(2)}) %collective-permute-start.43) | collective-permute-done | bytes 1440 | tf_op jit(solution)/shard_map/ppermute | solution.py:317
  150.7 3.9 %collective-permute-done.40 = bf16[176,512]{1,0:T(8,128)(2,1)S(1)} collective-permute-done((bf16[176,512]{1,0:T(8,128)(2,1)S(1)}, bf16[176,512]{1,0:T(8,128)(2,1)S(1)}, u32[]{:S(2)}, u32[]{:S(2)}) %collective-permute-start.40) | collective-permute-done | bytes 180256 | tf_op jit(solution)/shard_map/ppermute | solution.py:309
  (115 shorter events, 41.2 us)
Async XLA Ops:
  8.7 19.8 %collective-permute-start = (bf16[2,64,2048]{2,1,0:T(8,128)(2,1)S(1)}, bf16[2,64,2048]{2,1,0:T(8,128)(2,1)S(1)}, u32[]{:S(2)}, u32[]{:S(2)}) collective-permute-start(bf16[2,64,2048]{2,1,0:T(8,128)(2,1)S(1)} %pad_maximum_fusion), channel_id=1, source_target_pairs={{0,16},{16,0},{1,17},{17,1},{2,18},{18,2},{3,19},{19,3},{4,20},{20... | collective-permute-start | bytes 1572872 | tf_op jit(solution)/shard_map/ppermute | solution.py:248
  12.3 15.5 %collective-permute-start.8 = (bf16[64,2048]{1,0:T(8,128)(2,1)S(1)}, bf16[64,2048]{1,0:T(8,128)(2,1)S(1)}, u32[]{:S(2)}, u32[]{:S(2)}) collective-permute-start(bf16[64,2048]{1,0:T(8,128)(2,1)S(1)} %collective-permute-done.7.refs_0_), channel_id=1, source_target_pairs={{0,16},{16,0},{1,17},{17,1},{2,18},{18,2},{3,19},{19,3},{4,20},{20... | collective-permute-start | bytes 786440 | tf_op jit(solution)/shard_map/ppermute | solution.py:262
  14.9 15.2 %collective-permute-start.18 = (bf16[352,512]{1,0:T(8,128)(2,1)S(1)}, bf16[352,512]{1,0:T(8,128)(2,1)S(1)}, u32[]{:S(2)}, u32[]{:S(2)}) collective-permute-start(bf16[352,512]{1,0:T(8,128)(2,1)S(1)} %pad_maximum_fusion.3.own.refs_6_), channel_id=1, source_target_pairs={{0,4},{4,0},{8,12},{12,8},{1,5},{5,1},{9,13},{13,9},{2,6},{6,2},{1... | collective-permute-start | bytes 1081352 | tf_op jit(solution)/shard_map/ppermute | solution.py:246
  17.4 13.3 %collective-permute-start.19 = (bf16[352,512]{1,0:T(8,128)(2,1)S(1)}, bf16[352,512]{1,0:T(8,128)(2,1)S(1)}, u32[]{:S(2)}, u32[]{:S(2)}) collective-permute-start(bf16[352,512]{1,0:T(8,128)(2,1)S(1)} %pad_maximum_fusion.3.own.refs_6_), channel_id=1, source_target_pairs={{4,8},{8,4},{5,9},{9,5},{6,10},{10,6},{7,11},{11,7},{20,24},{24,20... | collective-permute-start | bytes 1081352 | tf_op jit(solution)/shard_map/ppermute | solution.py:247
  18.1 16.9 %collective-permute-start.13 = (bf16[352,512]{1,0:T(8,128)(2,1)S(1)}, bf16[352,512]{1,0:T(8,128)(2,1)S(1)}, u32[]{:S(2)}, u32[]{:S(2)}) collective-permute-start(bf16[352,512]{1,0:T(8,128)(2,1)S(1)} %pad_maximum_fusion.2.own.refs_0_), channel_id=1, source_target_pairs={{0,4},{4,0},{8,12},{12,8},{1,5},{5,1},{9,13},{13,9},{2,6},{6,2},{1... | collective-permute-start | bytes 1081352 | tf_op jit(solution)/shard_map/ppermute | solution.py:244
  28.6 14.9 %collective-permute-start.1 = (bf16[2,64,2048]{2,1,0:T(8,128)(2,1)S(1)}, bf16[2,64,2048]{2,1,0:T(8,128)(2,1)S(1)}, u32[]{:S(2)}, u32[]{:S(2)}) collective-permute-start(bf16[2,64,2048]{2,1,0:T(8,128)(2,1)S(1)} %collective-permute-done.refs_0_), channel_id=1, source_target_pairs={{0,2},{2,0},{1,3},{3,1},{4,6},{6,4},{5,7},{7,5},{8,10},{10,8},{9,1... | collective-permute-start | bytes 1572872 | tf_op jit(solution)/shard_map/ppermute | solution.py:256
  30.1 22.3 %collective-permute-start.9 = (bf16[2,64,2048]{2,1,0:T(8,128)(2,1)S(1)}, bf16[2,64,2048]{2,1,0:T(8,128)(2,1)S(1)}, u32[]{:S(2)}, u32[]{:S(2)}) collective-permute-start(bf16[2,64,2048]{2,1,0:T(8,128)(2,1)S(1)} %pad_maximum_fusion.1), channel_id=1, source_target_pairs={{0,2},{2,0},{1,3},{3,1},{4,6},{6,4},{5,7},{7,5},{8,10},{10,8},{9,1... | collective-permute-start | bytes 1572872 | tf_op jit(solution)/shard_map/ppermute | solution.py:264
  41.0 11.4 %collective-permute-start.16 = (bf16[352,512]{1,0:T(8,128)(2,1)S(1)}, bf16[352,512]{1,0:T(8,128)(2,1)S(1)}, u32[]{:S(2)}, u32[]{:S(2)}) collective-permute-start(bf16[352,512]{1,0:T(8,128)(2,1)S(1)} %collective-permute-done.13.pair.refs_1_), channel_id=1, source_target_pairs={{4,8},{8,4},{5,9},{9,5},{6,10},{10,6},{7,11},{11,7},{20,24},{24,20... | collective-permute-start | bytes 1081352 | tf_op jit(solution)/shard_map/ppermute | solution.py:252
  41.7 11.3 %collective-permute-start.6 = (bf16[352,512]{1,0:T(8,128)(2,1)S(1)}, bf16[352,512]{1,0:T(8,128)(2,1)S(1)}, u32[]{:S(2)}, u32[]{:S(2)}) collective-permute-start(bf16[352,512]{1,0:T(8,128)(2,1)S(1)} %collective-permute-done.4.d1.refs_5_), channel_id=1, source_target_pairs={{4,8},{8,4},{5,9},{9,5},{6,10},{10,6},{7,11},{11,7},{20,24},{24,20... | collective-permute-start | bytes 1081352 | tf_op jit(solution)/shard_map/ppermute | solution.py:260
  42.4 13.4 %collective-permute-start.2 = (bf16[2,64,2048]{2,1,0:T(8,128)(2,1)S(1)}, bf16[2,64,2048]{2,1,0:T(8,128)(2,1)S(1)}, u32[]{:S(2)}, u32[]{:S(2)}) collective-permute-start(bf16[2,64,2048]{2,1,0:T(8,128)(2,1)S(1)} %collective-permute-done.refs_0_), channel_id=1, source_target_pairs={{0,1},{1,0},{2,3},{3,2},{4,5},{5,4},{6,7},{7,6},{8,9},{9,8},{10,11... | collective-permute-start | bytes 1572872 | tf_op jit(solution)/shard_map/ppermute | solution.py:258
  53.0 27.0 %collective-permute-start.20 = (bf16[352,512]{1,0:T(8,128)(2,1)S(1)}, bf16[352,512]{1,0:T(8,128)(2,1)S(1)}, u32[]{:S(2)}, u32[]{:S(2)}) collective-permute-start(bf16[352,512]{1,0:T(8,128)(2,1)S(1)} %collective-permute-done.19.mid_i.refs_8_), channel_id=1, source_target_pairs={{4,0},{8,12},{5,1},{9,13},{6,2},{10,14},{7,3},{11,15},{20,16},{24,... | collective-permute-start | bytes 1081352 | tf_op jit(solution)/shard_map/ppermute | solution.py:255
  54.5 33.3 %collective-permute-start.22 = (bf16[352,512]{1,0:T(8,128)(2,1)S(1)}, bf16[352,512]{1,0:T(8,128)(2,1)S(1)}, u32[]{:S(2)}, u32[]{:S(2)}) collective-permute-start(bf16[352,512]{1,0:T(8,128)(2,1)S(1)} %collective-permute-done.21.far_i.refs_10_), channel_id=1, source_target_pairs={{4,0},{8,12},{5,1},{9,13},{6,2},{10,14},{7,3},{11,15},{20,16},{24,... | collective-permute-start | bytes 1081352 | tf_op jit(solution)/shard_map/ppermute | solution.py:263
  55.8 39.7 %collective-permute-start.15 = (bf16[352,512]{1,0:T(8,128)(2,1)S(1)}, bf16[352,512]{1,0:T(8,128)(2,1)S(1)}, u32[]{:S(2)}, u32[]{:S(2)}) collective-permute-start(bf16[352,512]{1,0:T(8,128)(2,1)S(1)} %collective-permute-done.14.mid_i.refs_2_), channel_id=1, source_target_pairs={{4,0},{8,12},{5,1},{9,13},{6,2},{10,14},{7,3},{11,15},{20,16},{24,... | collective-permute-start | bytes 1081352 | tf_op jit(solution)/shard_map/ppermute | solution.py:253
  57.1 45.9 %collective-permute-start.17 = (bf16[352,512]{1,0:T(8,128)(2,1)S(1)}, bf16[352,512]{1,0:T(8,128)(2,1)S(1)}, u32[]{:S(2)}, u32[]{:S(2)}) collective-permute-start(bf16[352,512]{1,0:T(8,128)(2,1)S(1)} %collective-permute-done.16.far_i.refs_4_), channel_id=1, source_target_pairs={{4,0},{8,12},{5,1},{9,13},{6,2},{10,14},{7,3},{11,15},{20,16},{24,... | collective-permute-start | bytes 1081352 | tf_op jit(solution)/shard_map/ppermute | solution.py:259
  58.4 49.0 %collective-permute-start.10 = (bf16[64,2048]{1,0:T(8,128)(2,1)S(1)}, bf16[64,2048]{1,0:T(8,128)(2,1)S(1)}, u32[]{:S(2)}, u32[]{:S(2)}) collective-permute-start(bf16[64,2048]{1,0:T(8,128)(2,1)S(1)} %collective-permute-done.7.refs_0_), channel_id=1, source_target_pairs={{0,1},{1,0},{2,3},{3,2},{4,5},{5,4},{6,7},{7,6},{8,9},{9,8},{10,11... | collective-permute-start | bytes 786440 | tf_op jit(solution)/shard_map/ppermute | solution.py:267
  80.1 27.4 %collective-permute-start.11 = (bf16[64,2048]{1,0:T(8,128)(2,1)S(1)}, bf16[64,2048]{1,0:T(8,128)(2,1)S(1)}, u32[]{:S(2)}, u32[]{:S(2)}) collective-permute-start(bf16[64,2048]{1,0:T(8,128)(2,1)S(1)} %get-tuple-element.54.refs_1_), channel_id=1, source_target_pairs={{0,1},{1,0},{2,3},{3,2},{4,5},{5,4},{6,7},{7,6},{8,9},{9,8},{10,11... | collective-permute-start | bytes 786440 | tf_op jit(solution)/shard_map/ppermute | solution.py:267
  87.8 18.2 %collective-permute-start.26 = (bf16[352,256]{1,0:T(8,128)(2,1)S(1)}, bf16[352,256]{1,0:T(8,128)(2,1)S(1)}, u32[]{:S(2)}, u32[]{:S(2)}) collective-permute-start(bf16[352,256]{1,0:T(8,128)(2,1)S(1)} %shard_map.83), channel_id=1, source_target_pairs={{4,0},{8,12},{5,1},{9,13},{6,2},{10,14},{7,3},{11,15},{20,16},{24,... | collective-permute-start | bytes 540680 | tf_op jit(solution)/shard_map/ppermute | solution.py:288
  95.5 13.3 %collective-permute-start.37 = (bf16[2,176,512]{2,1,0:T(8,128)(2,1)S(1)}, bf16[2,176,512]{2,1,0:T(8,128)(2,1)S(1)}, u32[]{:S(2)}, u32[]{:S(2)}) collective-permute-start(bf16[2,176,512]{2,1,0:T(8,128)(2,1)S(1)} %get-tuple-element.44), channel_id=1, source_target_pairs={{0,4},{12,8},{1,5},{13,9},{2,6},{14,10},{3,7},{15,11},{16,20},{28,... | collective-permute-start | bytes 1081352 | tf_op jit(solution)/shard_map/ppermute | solution.py:278
  110.9 13.9 %collective-permute-start.35 = (bf16[2,176,512]{2,1,0:T(8,128)(2,1)S(1)}, bf16[2,176,512]{2,1,0:T(8,128)(2,1)S(1)}, u32[]{:S(2)}, u32[]{:S(2)}) collective-permute-start(bf16[2,176,512]{2,1,0:T(8,128)(2,1)S(1)} %shard_map.91), channel_id=1, source_target_pairs={{4,8},{8,4},{5,9},{9,5},{6,10},{10,6},{7,11},{11,7},{20,24},{24,20... | collective-permute-start | bytes 1081352 | tf_op jit(solution)/shard_map/ppermute | solution.py:291
  117.6 20.1 %collective-permute-start.23 = (bf16[2,128,1024]{2,1,0:T(8,128)(2,1)S(1)}, bf16[2,128,1024]{2,1,0:T(8,128)(2,1)S(1)}, u32[]{:S(2)}, u32[]{:S(2)}) collective-permute-start(bf16[2,128,1024]{2,1,0:T(8,128)(2,1)S(1)} %get-tuple-element.30), channel_id=1, source_target_pairs={{0,1},{1,0},{2,3},{3,2},{4,5},{5,4},{6,7},{7,6},{8,9},{9,8},{10,11... | collective-permute-start | bytes 1572872 | tf_op jit(solution)/shard_map/ppermute | solution.py:300
  117.8 20.0 %collective-permute-start.30 = (bf16[128,1024]{1,0:T(8,128)(2,1)S(1)}, bf16[128,1024]{1,0:T(8,128)(2,1)S(1)}, u32[]{:S(2)}, u32[]{:S(2)}) collective-permute-start(bf16[128,1024]{1,0:T(8,128)(2,1)S(1)} %get-tuple-element.36), channel_id=1, source_target_pairs={{0,16},{16,0},{1,17},{17,1},{2,18},{18,2},{3,19},{19,3},{4,20},{20... | collective-permute-start | bytes 786440 | tf_op jit(solution)/shard_map/ppermute | solution.py:323
  119.4 20.1 %collective-permute-start.28 = (bf16[128,1024]{1,0:T(8,128)(2,1)S(1)}, bf16[128,1024]{1,0:T(8,128)(2,1)S(1)}, u32[]{:S(2)}, u32[]{:S(2)}) collective-permute-start(bf16[128,1024]{1,0:T(8,128)(2,1)S(1)} %get-tuple-element.34), channel_id=1, source_target_pairs={{0,16},{16,0},{1,17},{17,1},{2,18},{18,2},{3,19},{19,3},{4,20},{20... | collective-permute-start | bytes 786440 | tf_op jit(solution)/shard_map/ppermute | solution.py:323
  120.0 11.7 %collective-permute-start.39 = (bf16[176,512]{1,0:T(8,128)(2,1)S(1)}, bf16[176,512]{1,0:T(8,128)(2,1)S(1)}, u32[]{:S(2)}, u32[]{:S(2)}) collective-permute-start(bf16[176,512]{1,0:T(8,128)(2,1)S(1)} %get-tuple-element.46), channel_id=1, source_target_pairs={{0,4},{4,0},{8,12},{12,8},{1,5},{5,1},{9,13},{13,9},{2,6},{6,2},{1... | collective-permute-start | bytes 540680 | tf_op jit(solution)/shard_map/ppermute | solution.py:307
  138.0 11.9 %collective-permute-start.31 = (bf16[128,1024]{1,0:T(8,128)(2,1)S(1)}, bf16[128,1024]{1,0:T(8,128)(2,1)S(1)}, u32[]{:S(2)}, u32[]{:S(2)}) collective-permute-start(bf16[128,1024]{1,0:T(8,128)(2,1)S(1)} %shard_map.88.a), channel_id=1, source_target_pairs={{0,2},{2,0},{1,3},{3,1},{4,6},{6,4},{5,7},{7,5},{8,10},{10,8},{9,1... | collective-permute-start | bytes 786440 | tf_op jit(solution)/shard_map/ppermute | solution.py:325
  (25 other events, 216.6 us)

commit v3 on v2

--- a/solution.py
+++ b/solution.py
@@ -130,12 +130,12 @@
     pre[...] = project((own[...], pair[...], either(inner, mid_i, mid_o), either(inner, far_i, far_o)), xs)
     gate = pre[:part, :]
     hidden = (gate * jax.nn.sigmoid(gate) * pre[part:, :]).astype(BF16)
-    near[0] = dot(hidden, gs[0])
-    near[1] = dot(hidden, gs[1])
     for p in range(2):
         block = dot(hidden, gs[2 + p])
         far[p] = block
         far_cast[p] = block.astype(BF16)
+    near[0] = dot(hidden, gs[0])
+    near[1] = dot(hidden, gs[1])
 
 
 def pair_kernel(*refs):
@@ -194,6 +194,14 @@
 def near_kernel(near, got, owned, paired_sum):
     owned[...] = near[0] + got[0].astype(F32)
     paired_sum[...] = (near[1] + got[1].astype(F32)).astype(BF16)
+
+
+def pair_add_kernel(near, got, out):
+    out[...] = (near[1] + got[...].astype(F32)).astype(BF16)
+
+
+def own_add_kernel(near, got, last, out):
+    out[...] = (near[0] + got[...].astype(F32) + last[...].astype(F32)).astype(BF16)
 
 
 def add_kernel(a, b, out):
@@ -273,11 +281,15 @@
     for c in range(2):
         outs = [like((2 * parts[c], count), F32)] + [like((2, parts[c], depth), d) for d in (F32, F32, BF16)]
         fronts.append(call(front_kernel, outs, flops=6 * count * width * parts[c])(xs, gs, *gu_sets[c]))
-    gots = []
-    for c in range(2):
-        got = lax.ppermute(fronts[c][3], "fs", INWARD)
-        far = fronts[c][2]
-        gots += call(add_kernel, [like(far.shape, BF16)])(far, got)
+    far, cast = fronts[0][2:]
+    got = lax.ppermute(cast, "fs", INWARD)
+    (far,) = call(add_kernel, [like(far.shape, BF16)])(far, got)
+    from_a = lax.ppermute(far, "fs", MIDDLE)
+    far, cast = fronts[1][2:]
+    got = lax.ppermute(cast, "fs", INWARD)
+    far_in, far_out = call(add_halves_kernel, [like(far.shape[1:], BF16)] * 2)(far, got)
+    from_bc = lax.ppermute(far_out, "fs", MIDDLE)
+    from_bb = lax.ppermute(far_in, "fs", MIDDLE)
 
     down_pieces = (down_h, p1d, p2d, p3d)
     hid_gots = [None, None]
@@ -288,7 +300,6 @@
         hid_gots[group] = lax.ppermute(pair_hid, "fs", OUTWARD)
     (own_hid,) = call(own_kernel, [like((half, count), F32)], flops=2 * count * width * half)(gs, *down_pieces)
 
-    gots = [lax.ppermute(gots[c], "fs", MIDDLE) for c in range(2)]
     halves = [None, None]
     for group in (1, 0):
         keep, give = call(
@@ -300,12 +311,13 @@
         got = lax.ppermute(give, "tp", OVER_CORE)
         halves[group] = call(add_halves_kernel, [like(keep.shape[1:], BF16)] * 2)(keep, got)
 
-    finals = []
-    for c in range(2):
-        block = gots[c].shape[1:]
-        owned, paired_sum = call(near_kernel, [like(block, F32), like(block, BF16)])(fronts[c][1], gots[c])
-        last = lax.ppermute(paired_sum, "fs", OUTER_PAIRS)
-        finals += call(add_kernel, [like(block, BF16)])(owned, last)
+    near_a, near_b = fronts[0][1], fronts[1][1]
+    owned, paired_a = call(near_kernel, [like(near_a.shape[1:], d) for d in (F32, BF16)])(near_a, from_a)
+    (paired_b,) = call(pair_add_kernel, [like(near_b.shape[1:], BF16)])(near_b, from_bc)
+    last_a = lax.ppermute(paired_a, "fs", OUTER_PAIRS)
+    last_b = lax.ppermute(paired_b, "fs", OUTER_PAIRS)
+    finals = call(add_kernel, [like(owned.shape, BF16)])(owned, last_a)
+    finals += call(own_add_kernel, [like(paired_b.shape, BF16)])(near_b, from_bb, last_b)
     peers = [lax.ppermute(finals[c], "rep", SWAP) for c in range(2)]
     final_own, peers = jnp.concatenate(finals, 0), jnp.concatenate(peers, 0)
     low = jnp.where(y == 0, final_own, peers)

time: 158 us -> 159 us (level)
  waiting for transfers between devices: 80.4 us -> 83.1 us
  starting transfers between devices: 61 us -> 59.4 us
    ppermute x1, waiting for transfers between devices: 5.02 us -> 21.2 us  [paired_body(): p4a = lax.ppermute(p2a, 'fs', OUTWARD)]
    ppermute x1, waiting for transfers between devices: 21.2 us -> 5.02 us  [paired_body(): p4b = lax.ppermute(p2b, 'fs', OUTWARD)]
    ppermute x2, waiting for transfers between devices: 4.69 us -> 6.72 us  [paired_body(): hid_gots[group] = lax.ppermute(pair_hid, 'fs', OUTWARD)]
    ppermute x1, waiting for transfers between devices: 6.06 us -> 7.72 us  [paired_body(): p5a = lax.ppermute(p3a, 'fs', OUTWARD)]
    ppermute x1, waiting for transfers between devices: 7.72 us -> 6.06 us  [paired_body(): p5b = lax.ppermute(p3b, 'fs', OUTWARD)]
    ppermute x6 -> x7, starting transfers between devices: 16 us -> 15.1 us  [the longest x1 8.74 us: paired_body(): last_b = lax.ppermute(paired_b, 'fs', OUTER_PAIRS)]
    ppermute x6 -> x7, waiting for transfers between devices: 5.28 us -> 5.86 us  [the longest x1 3.93 us: paired_body(): last_b = lax.ppermute(paired_b, 'fs', OUTER_PAIRS)]
  transfers between devices with their start and end apart: 45 -> 46, of which waited for: 14 -> 15; matrix products, arithmetic and copies ran while one was open for 4% -> 3% of each run, Pallas kernels for 4% -> 4%
where the time goes in v3:
time: 159 us; the launch traced here: 158 us
  waiting for transfers between devices  83.1 us (52%)
  starting transfers between devices  59.4 us (37%)
  Pallas kernels  7.79 us (5%)
  local copies, waits for them, and re-layouts  4.2 us (3%)
  other arithmetic  2.43 us (2%)
    ppermute x1, waiting for transfers between devices, paired_body(): p4a = lax.ppermute(p2a, 'fs', OUTWARD)  21.2 us
    ppermute x1, waiting for transfers between devices, paired_body(): gp_x = lax.ppermute(jnp.stack([gp[0], gp[4]], 0), 'tp', OVER_X)  8.97 us
    ppermute x1, starting transfers between devices, paired_body(): last_b = lax.ppermute(paired_b, 'fs', OUTER_PAIRS)  8.74 us
    pallas_call x21, Pallas kernels, inner_call(): pl.pallas_call(kernel, out_shape=outs, in_specs=[pl.BlockSpec(memory_spac...  7.79 us
    ppermute x1, waiting for transfers between devices, paired_body(): p5a = lax.ppermute(p3a, 'fs', OUTWARD)  7.72 us
    ppermute x1, waiting for transfers between devices, paired_body(): gp[4] = lax.ppermute(gp[0], 'rep', SWAP)  6.78 us
    ppermute x2, waiting for transfers between devices, paired_body(): hid_gots[group] = lax.ppermute(pair_hid, 'fs', OUTWARD)  6.72 us
    ppermute x1, waiting for transfers between devices, paired_body(): p5b = lax.ppermute(p3b, 'fs', OUTWARD)  6.06 us
  transfers between devices with their start and end apart: 46, of which 15 were waited for; matrix products, arithmetic and copies ran while one was open for 3% of the time, Pallas kernels for 4%

profile of v3, /device:TPU:0, one launch (start us, length us, event | category | flops | bytes accessed | tf_op | source)
XLA Modules:
  0.0 158.1 jit_solution(7408977911798871338)
XLA Ops:
  1.7 5.0 %collective-permute-start.7 = (bf16[64,2048]{1,0:T(8,128)(2,1)S(1)}, bf16[64,2048]{1,0:T(8,128)(2,1)S(1)}, u32[]{:S(2)}, u32[]{:S(2)}) collective-permute-start(bf16[64,2048]{1,0:T(8,128)(2,1)S(1)} %constant_dynamic-slice_fusion.1), channel_id=1, source_target_pairs={{0,4},{12,8},{1,5},{13,9},{2,6},{14,10},{3,7},{15,11},{16,20},{28,... | collective-permute-start | bytes 786440 | tf_op jit(solution)/shard_map/ppermute | solution.py:259
  8.7 1.6 %collective-permute-start = (bf16[2,64,2048]{2,1,0:T(8,128)(2,1)S(1)}, bf16[2,64,2048]{2,1,0:T(8,128)(2,1)S(1)}, u32[]{:S(2)}, u32[]{:S(2)}) collective-permute-start(bf16[2,64,2048]{2,1,0:T(8,128)(2,1)S(1)} %pad_maximum_fusion), channel_id=1, source_target_pairs={{0,16},{16,0},{1,17},{17,1},{2,18},{18,2},{3,19},{19,3},{4,20},{20... | collective-permute-start | bytes 1572872 | tf_op jit(solution)/shard_map/ppermute | solution.py:256
  10.3 1.9 %collective-permute-done.7.refs_0_ = bf16[64,2048]{1,0:T(8,128)(2,1)S(1)} collective-permute-done((bf16[64,2048]{1,0:T(8,128)(2,1)S(1)}, bf16[64,2048]{1,0:T(8,128)(2,1)S(1)}, u32[]{:S(2)}, u32[]{:S(2)}) %collective-permute-start.7) | collective-permute-done | bytes 262176 | tf_op jit(solution)/shard_map/ppermute | solution.py:259
  14.9 2.5 %collective-permute-start.18 = (bf16[352,512]{1,0:T(8,128)(2,1)S(1)}, bf16[352,512]{1,0:T(8,128)(2,1)S(1)}, u32[]{:S(2)}, u32[]{:S(2)}) collective-permute-start(bf16[352,512]{1,0:T(8,128)(2,1)S(1)} %pad_maximum_fusion.3.own.refs_6_), channel_id=1, source_target_pairs={{0,4},{4,0},{8,12},{12,8},{1,5},{5,1},{9,13},{13,9},{2,6},{6,2},{1... | collective-permute-start | bytes 1081352 | tf_op jit(solution)/shard_map/ppermute | solution.py:254
  18.1 2.9 %collective-permute-start.13 = (bf16[352,512]{1,0:T(8,128)(2,1)S(1)}, bf16[352,512]{1,0:T(8,128)(2,1)S(1)}, u32[]{:S(2)}, u32[]{:S(2)}) collective-permute-start(bf16[352,512]{1,0:T(8,128)(2,1)S(1)} %pad_maximum_fusion.2.own.refs_0_), channel_id=1, source_target_pairs={{0,4},{4,0},{8,12},{12,8},{1,5},{5,1},{9,13},{13,9},{2,6},{6,2},{1... | collective-permute-start | bytes 1081352 | tf_op jit(solution)/shard_map/ppermute | solution.py:252
  21.0 6.8 %collective-permute-done.8.refs_0_ = bf16[64,2048]{1,0:T(8,128)(2,1)S(1)} collective-permute-done((bf16[64,2048]{1,0:T(8,128)(2,1)S(1)}, bf16[64,2048]{1,0:T(8,128)(2,1)S(1)}, u32[]{:S(2)}, u32[]{:S(2)}) %collective-permute-start.8) | collective-permute-done | bytes 262176 | tf_op jit(solution)/shard_map/ppermute | solution.py:270
  28.6 1.6 collective-permute-start.1
  30.7 4.4 %collective-permute-start.4 = (bf16[352,512]{1,0:T(8,128)(2,1)S(1)}, bf16[352,512]{1,0:T(8,128)(2,1)S(1)}, u32[]{:S(2)}, u32[]{:S(2)}) collective-permute-start(bf16[352,512]{1,0:T(8,128)(2,1)S(1)} %constant_dynamic-slice_fusion.d0.refs_4_), channel_id=1, source_target_pairs={{0,4},{12,8},{1,5},{13,9},{2,6},{14,10},{3,7},{15,11},{16,20},{28,... | collective-permute-start | bytes 1081352 | tf_op jit(solution)/shard_map/ppermute | solution.py:257
  36.5 4.5 %collective-permute-done.4.d1.refs_5_ = bf16[352,512]{1,0:T(8,128)(2,1)S(1)} collective-permute-done((bf16[352,512]{1,0:T(8,128)(2,1)S(1)}, bf16[352,512]{1,0:T(8,128)(2,1)S(1)}, u32[]{:S(2)}, u32[]{:S(2)}) %collective-permute-start.4) | collective-permute-done | bytes 360480 | tf_op jit(solution)/shard_map/ppermute | solution.py:257
  43.4 9.0 %collective-permute-done.9 = bf16[2,64,2048]{2,1,0:T(8,128)(2,1)S(1)} collective-permute-done((bf16[2,64,2048]{2,1,0:T(8,128)(2,1)S(1)}, bf16[2,64,2048]{2,1,0:T(8,128)(2,1)S(1)}, u32[]{:S(2)}, u32[]{:S(2)}) %collective-permute-start.9) | collective-permute-done | bytes 524320 | tf_op jit(solution)/shard_map/ppermute | solution.py:272
  58.9 21.2 %collective-permute-done.15.mid_o.refs_3_ = bf16[352,512]{1,0:T(8,128)(2,1)S(1)} collective-permute-done((bf16[352,512]{1,0:T(8,128)(2,1)S(1)}, bf16[352,512]{1,0:T(8,128)(2,1)S(1)}, u32[]{:S(2)}, u32[]{:S(2)}) %collective-permute-start.15) | collective-permute-done | bytes 360480 | tf_op jit(solution)/shard_map/ppermute | solution.py:261
  80.1 7.7 %collective-permute-done.17.far_o.refs_5_ = bf16[352,512]{1,0:T(8,128)(2,1)S(1)} collective-permute-done((bf16[352,512]{1,0:T(8,128)(2,1)S(1)}, bf16[352,512]{1,0:T(8,128)(2,1)S(1)}, u32[]{:S(2)}, u32[]{:S(2)}) %collective-permute-start.17) | collective-permute-done | bytes 360480 | tf_op jit(solution)/shard_map/ppermute | solution.py:267
  90.5 5.0 %collective-permute-done.20.mid_o.refs_9_ = bf16[352,512]{1,0:T(8,128)(2,1)S(1)} collective-permute-done((bf16[352,512]{1,0:T(8,128)(2,1)S(1)}, bf16[352,512]{1,0:T(8,128)(2,1)S(1)}, u32[]{:S(2)}, u32[]{:S(2)}) %collective-permute-start.20) | collective-permute-done | bytes 360480 | tf_op jit(solution)/shard_map/ppermute | solution.py:263
  97.0 6.1 %collective-permute-done.22.far_o.refs_11_ = bf16[352,512]{1,0:T(8,128)(2,1)S(1)} collective-permute-done((bf16[352,512]{1,0:T(8,128)(2,1)S(1)}, bf16[352,512]{1,0:T(8,128)(2,1)S(1)}, u32[]{:S(2)}, u32[]{:S(2)}) %collective-permute-start.22) | collective-permute-done | bytes 360480 | tf_op jit(solution)/shard_map/ppermute | solution.py:271
  109.5 6.7 %collective-permute-done.12.got = bf16[352,256]{1,0:T(8,128)(2,1)S(1)} collective-permute-done((bf16[352,256]{1,0:T(8,128)(2,1)S(1)}, bf16[352,256]{1,0:T(8,128)(2,1)S(1)}, u32[]{:S(2)}, u32[]{:S(2)}) %collective-permute-start.12) | collective-permute-done | bytes 180256 | tf_op jit(solution)/shard_map/ppermute | solution.py:300
  119.3 1.6 %collective-permute-start.30 = (bf16[128,1024]{1,0:T(8,128)(2,1)S(1)}, bf16[128,1024]{1,0:T(8,128)(2,1)S(1)}, u32[]{:S(2)}, u32[]{:S(2)}) collective-permute-start(bf16[128,1024]{1,0:T(8,128)(2,1)S(1)} %get-tuple-element.36), channel_id=1, source_target_pairs={{0,16},{16,0},{1,17},{17,1},{2,18},{18,2},{3,19},{19,3},{4,20},{20... | collective-permute-start | bytes 786440 | tf_op jit(solution)/shard_map/ppermute | solution.py:335
  121.4 8.7 %collective-permute-start.40 = (bf16[176,512]{1,0:T(8,128)(2,1)S(1)}, bf16[176,512]{1,0:T(8,128)(2,1)S(1)}, u32[]{:S(2)}, u32[]{:S(2)}) collective-permute-start(bf16[176,512]{1,0:T(8,128)(2,1)S(1)} %shard_map.95), channel_id=1, source_target_pairs={{0,4},{4,0},{8,12},{12,8},{1,5},{5,1},{9,13},{13,9},{2,6},{6,2},{1... | collective-permute-start | bytes 540680 | tf_op jit(solution)/shard_map/ppermute | solution.py:318
  131.6 3.9 %collective-permute-done.40.last = bf16[176,512]{1,0:T(8,128)(2,1)S(1)} collective-permute-done((bf16[176,512]{1,0:T(8,128)(2,1)S(1)}, bf16[176,512]{1,0:T(8,128)(2,1)S(1)}, u32[]{:S(2)}, u32[]{:S(2)}) %collective-permute-start.40) | collective-permute-done | bytes 180256 | tf_op jit(solution)/shard_map/ppermute | solution.py:318
  135.6 1.9 %collective-permute-done.36.b = bf16[176,512]{1,0:T(8,128)(2,1)S(1)} collective-permute-done((bf16[176,512]{1,0:T(8,128)(2,1)S(1)}, bf16[176,512]{1,0:T(8,128)(2,1)S(1)}, u32[]{:S(2)}, u32[]{:S(2)}) %collective-permute-start.36) | collective-permute-done | bytes 180256 | tf_op jit(solution)/shard_map/ppermute | solution.py:317
  137.7 1.9 %collective-permute-start.43 = (f32[1,352]{1,0:T(1,128)S(1)}, f32[1,352]{1,0:T(1,128)S(1)}, u32[]{:S(2)}, u32[]{:S(2)}) collective-permute-start(f32[1,352]{1,0:T(1,128)S(1)} %reshape_broadcast_in_dim.3), channel_id=1, source_target_pairs={{0,4},{4,0},{8,12},{12,8},{1,5},{5,1},{9,13},{13,9},{2,6},{6,2},{1... | collective-permute-start | bytes 4232 | tf_op jit(solution)/shard_map/ppermute | solution.py:328
  139.8 1.6 collective-permute-start.31
  142.0 2.0 %collective-permute-start.44 = (f32[1,352]{1,0:T(1,128)S(1)}, f32[1,352]{1,0:T(1,128)S(1)}, u32[]{:S(2)}, u32[]{:S(2)}) collective-permute-start(f32[1,352]{1,0:T(1,128)S(1)} %reshape_add_fusion), channel_id=1, source_target_pairs={{0,12},{12,0},{4,8},{8,4},{1,13},{13,1},{5,9},{9,5},{2,14},{14,2},... | collective-permute-start | bytes 4232 | tf_op jit(solution)/shard_map/ppermute | solution.py:329
  144.1 3.3 %collective-permute-done.44 = f32[1,352]{1,0:T(1,128)S(1)} collective-permute-done((f32[1,352]{1,0:T(1,128)S(1)}, f32[1,352]{1,0:T(1,128)S(1)}, u32[]{:S(2)}, u32[]{:S(2)}) %collective-permute-start.44) | collective-permute-done | bytes 1440 | tf_op jit(solution)/shard_map/ppermute | solution.py:329
  152.5 3.1 %collective-permute-done.41 = bf16[176,512]{1,0:T(8,128)(2,1)S(1)} collective-permute-done((bf16[176,512]{1,0:T(8,128)(2,1)S(1)}, bf16[176,512]{1,0:T(8,128)(2,1)S(1)}, u32[]{:S(2)}, u32[]{:S(2)}) %collective-permute-start.41) | collective-permute-done | bytes 180256 | tf_op jit(solution)/shard_map/ppermute | solution.py:321
  (117 shorter events, 41.9 us)
Async XLA Ops:
  8.7 19.8 %collective-permute-start = (bf16[2,64,2048]{2,1,0:T(8,128)(2,1)S(1)}, bf16[2,64,2048]{2,1,0:T(8,128)(2,1)S(1)}, u32[]{:S(2)}, u32[]{:S(2)}) collective-permute-start(bf16[2,64,2048]{2,1,0:T(8,128)(2,1)S(1)} %pad_maximum_fusion), channel_id=1, source_target_pairs={{0,16},{16,0},{1,17},{17,1},{2,18},{18,2},{3,19},{19,3},{4,20},{20... | collective-permute-start | bytes 1572872 | tf_op jit(solution)/shard_map/ppermute | solution.py:256
  12.3 15.5 %collective-permute-start.8 = (bf16[64,2048]{1,0:T(8,128)(2,1)S(1)}, bf16[64,2048]{1,0:T(8,128)(2,1)S(1)}, u32[]{:S(2)}, u32[]{:S(2)}) collective-permute-start(bf16[64,2048]{1,0:T(8,128)(2,1)S(1)} %collective-permute-done.7.refs_0_), channel_id=1, source_target_pairs={{0,16},{16,0},{1,17},{17,1},{2,18},{18,2},{3,19},{19,3},{4,20},{20... | collective-permute-start | bytes 786440 | tf_op jit(solution)/shard_map/ppermute | solution.py:270
  14.9 15.2 %collective-permute-start.18 = (bf16[352,512]{1,0:T(8,128)(2,1)S(1)}, bf16[352,512]{1,0:T(8,128)(2,1)S(1)}, u32[]{:S(2)}, u32[]{:S(2)}) collective-permute-start(bf16[352,512]{1,0:T(8,128)(2,1)S(1)} %pad_maximum_fusion.3.own.refs_6_), channel_id=1, source_target_pairs={{0,4},{4,0},{8,12},{12,8},{1,5},{5,1},{9,13},{13,9},{2,6},{6,2},{1... | collective-permute-start | bytes 1081352 | tf_op jit(solution)/shard_map/ppermute | solution.py:254
  17.4 13.3 %collective-permute-start.19 = (bf16[352,512]{1,0:T(8,128)(2,1)S(1)}, bf16[352,512]{1,0:T(8,128)(2,1)S(1)}, u32[]{:S(2)}, u32[]{:S(2)}) collective-permute-start(bf16[352,512]{1,0:T(8,128)(2,1)S(1)} %pad_maximum_fusion.3.own.refs_6_), channel_id=1, source_target_pairs={{4,8},{8,4},{5,9},{9,5},{6,10},{10,6},{7,11},{11,7},{20,24},{24,20... | collective-permute-start | bytes 1081352 | tf_op jit(solution)/shard_map/ppermute | solution.py:255
  18.1 16.9 %collective-permute-start.13 = (bf16[352,512]{1,0:T(8,128)(2,1)S(1)}, bf16[352,512]{1,0:T(8,128)(2,1)S(1)}, u32[]{:S(2)}, u32[]{:S(2)}) collective-permute-start(bf16[352,512]{1,0:T(8,128)(2,1)S(1)} %pad_maximum_fusion.2.own.refs_0_), channel_id=1, source_target_pairs={{0,4},{4,0},{8,12},{12,8},{1,5},{5,1},{9,13},{13,9},{2,6},{6,2},{1... | collective-permute-start | bytes 1081352 | tf_op jit(solution)/shard_map/ppermute | solution.py:252
  28.6 14.9 %collective-permute-start.1 = (bf16[2,64,2048]{2,1,0:T(8,128)(2,1)S(1)}, bf16[2,64,2048]{2,1,0:T(8,128)(2,1)S(1)}, u32[]{:S(2)}, u32[]{:S(2)}) collective-permute-start(bf16[2,64,2048]{2,1,0:T(8,128)(2,1)S(1)} %collective-permute-done.refs_0_), channel_id=1, source_target_pairs={{0,2},{2,0},{1,3},{3,1},{4,6},{6,4},{5,7},{7,5},{8,10},{10,8},{9,1... | collective-permute-start | bytes 1572872 | tf_op jit(solution)/shard_map/ppermute | solution.py:264
  30.1 22.3 %collective-permute-start.9 = (bf16[2,64,2048]{2,1,0:T(8,128)(2,1)S(1)}, bf16[2,64,2048]{2,1,0:T(8,128)(2,1)S(1)}, u32[]{:S(2)}, u32[]{:S(2)}) collective-permute-start(bf16[2,64,2048]{2,1,0:T(8,128)(2,1)S(1)} %pad_maximum_fusion.1), channel_id=1, source_target_pairs={{0,2},{2,0},{1,3},{3,1},{4,6},{6,4},{5,7},{7,5},{8,10},{10,8},{9,1... | collective-permute-start | bytes 1572872 | tf_op jit(solution)/shard_map/ppermute | solution.py:272
  42.4 13.4 %collective-permute-start.2 = (bf16[2,64,2048]{2,1,0:T(8,128)(2,1)S(1)}, bf16[2,64,2048]{2,1,0:T(8,128)(2,1)S(1)}, u32[]{:S(2)}, u32[]{:S(2)}) collective-permute-start(bf16[2,64,2048]{2,1,0:T(8,128)(2,1)S(1)} %collective-permute-done.refs_0_), channel_id=1, source_target_pairs={{0,1},{1,0},{2,3},{3,2},{4,5},{5,4},{6,7},{7,6},{8,9},{9,8},{10,11... | collective-permute-start | bytes 1572872 | tf_op jit(solution)/shard_map/ppermute | solution.py:266
  53.0 27.0 %collective-permute-start.15 = (bf16[352,512]{1,0:T(8,128)(2,1)S(1)}, bf16[352,512]{1,0:T(8,128)(2,1)S(1)}, u32[]{:S(2)}, u32[]{:S(2)}) collective-permute-start(bf16[352,512]{1,0:T(8,128)(2,1)S(1)} %collective-permute-done.14.mid_i.refs_2_), channel_id=1, source_target_pairs={{4,0},{8,12},{5,1},{9,13},{6,2},{10,14},{7,3},{11,15},{20,16},{24,... | collective-permute-start | bytes 1081352 | tf_op jit(solution)/shard_map/ppermute | solution.py:261
  54.5 33.3 %collective-permute-start.17 = (bf16[352,512]{1,0:T(8,128)(2,1)S(1)}, bf16[352,512]{1,0:T(8,128)(2,1)S(1)}, u32[]{:S(2)}, u32[]{:S(2)}) collective-permute-start(bf16[352,512]{1,0:T(8,128)(2,1)S(1)} %collective-permute-done.16.far_i.refs_4_), channel_id=1, source_target_pairs={{4,0},{8,12},{5,1},{9,13},{6,2},{10,14},{7,3},{11,15},{20,16},{24,... | collective-permute-start | bytes 1081352 | tf_op jit(solution)/shard_map/ppermute | solution.py:267
  55.8 39.7 %collective-permute-start.20 = (bf16[352,512]{1,0:T(8,128)(2,1)S(1)}, bf16[352,512]{1,0:T(8,128)(2,1)S(1)}, u32[]{:S(2)}, u32[]{:S(2)}) collective-permute-start(bf16[352,512]{1,0:T(8,128)(2,1)S(1)} %collective-permute-done.19.mid_i.refs_8_), channel_id=1, source_target_pairs={{4,0},{8,12},{5,1},{9,13},{6,2},{10,14},{7,3},{11,15},{20,16},{24,... | collective-permute-start | bytes 1081352 | tf_op jit(solution)/shard_map/ppermute | solution.py:263
  57.1 45.9 %collective-permute-start.22 = (bf16[352,512]{1,0:T(8,128)(2,1)S(1)}, bf16[352,512]{1,0:T(8,128)(2,1)S(1)}, u32[]{:S(2)}, u32[]{:S(2)}) collective-permute-start(bf16[352,512]{1,0:T(8,128)(2,1)S(1)} %collective-permute-done.21.far_i.refs_10_), channel_id=1, source_target_pairs={{4,0},{8,12},{5,1},{9,13},{6,2},{10,14},{7,3},{11,15},{20,16},{24,... | collective-permute-start | bytes 1081352 | tf_op jit(solution)/shard_map/ppermute | solution.py:271
  58.4 49.0 %collective-permute-start.10 = (bf16[64,2048]{1,0:T(8,128)(2,1)S(1)}, bf16[64,2048]{1,0:T(8,128)(2,1)S(1)}, u32[]{:S(2)}, u32[]{:S(2)}) collective-permute-start(bf16[64,2048]{1,0:T(8,128)(2,1)S(1)} %collective-permute-done.7.refs_0_), channel_id=1, source_target_pairs={{0,1},{1,0},{2,3},{3,2},{4,5},{5,4},{6,7},{7,6},{8,9},{9,8},{10,11... | collective-permute-start | bytes 786440 | tf_op jit(solution)/shard_map/ppermute | solution.py:275
  80.1 27.4 %collective-permute-start.11 = (bf16[64,2048]{1,0:T(8,128)(2,1)S(1)}, bf16[64,2048]{1,0:T(8,128)(2,1)S(1)}, u32[]{:S(2)}, u32[]{:S(2)}) collective-permute-start(bf16[64,2048]{1,0:T(8,128)(2,1)S(1)} %get-tuple-element.54.refs_1_), channel_id=1, source_target_pairs={{0,1},{1,0},{2,3},{3,2},{4,5},{5,4},{6,7},{7,6},{8,9},{9,8},{10,11... | collective-permute-start | bytes 786440 | tf_op jit(solution)/shard_map/ppermute | solution.py:275
  87.8 18.2 %collective-permute-start.26 = (bf16[352,256]{1,0:T(8,128)(2,1)S(1)}, bf16[352,256]{1,0:T(8,128)(2,1)S(1)}, u32[]{:S(2)}, u32[]{:S(2)}) collective-permute-start(bf16[352,256]{1,0:T(8,128)(2,1)S(1)} %shard_map.83), channel_id=1, source_target_pairs={{4,0},{8,12},{5,1},{9,13},{6,2},{10,14},{7,3},{11,15},{20,16},{24,... | collective-permute-start | bytes 540680 | tf_op jit(solution)/shard_map/ppermute | solution.py:300
  95.5 13.3 %collective-permute-start.34 = (bf16[2,176,512]{2,1,0:T(8,128)(2,1)S(1)}, bf16[2,176,512]{2,1,0:T(8,128)(2,1)S(1)}, u32[]{:S(2)}, u32[]{:S(2)}) collective-permute-start(bf16[2,176,512]{2,1,0:T(8,128)(2,1)S(1)} %get-tuple-element.39), channel_id=1, source_target_pairs={{0,4},{12,8},{1,5},{13,9},{2,6},{14,10},{3,7},{15,11},{16,20},{28,... | collective-permute-start | bytes 1081352 | tf_op jit(solution)/shard_map/ppermute | solution.py:285
  104.4 13.3 %collective-permute-start.37 = (bf16[2,176,512]{2,1,0:T(8,128)(2,1)S(1)}, bf16[2,176,512]{2,1,0:T(8,128)(2,1)S(1)}, u32[]{:S(2)}, u32[]{:S(2)}) collective-permute-start(bf16[2,176,512]{2,1,0:T(8,128)(2,1)S(1)} %get-tuple-element.44), channel_id=1, source_target_pairs={{0,4},{12,8},{1,5},{13,9},{2,6},{14,10},{3,7},{15,11},{16,20},{28,... | collective-permute-start | bytes 1081352 | tf_op jit(solution)/shard_map/ppermute | solution.py:289
  107.3 11.8 %collective-permute-start.27 = (bf16[2,128,1024]{2,1,0:T(8,128)(2,1)S(1)}, bf16[2,128,1024]{2,1,0:T(8,128)(2,1)S(1)}, u32[]{:S(2)}, u32[]{:S(2)}) collective-permute-start(bf16[2,128,1024]{2,1,0:T(8,128)(2,1)S(1)} %get-tuple-element.33), channel_id=1, source_target_pairs={{0,1},{1,0},{2,3},{3,2},{4,5},{5,4},{6,7},{7,6},{8,9},{9,8},{10,11... | collective-permute-start | bytes 1572872 | tf_op jit(solution)/shard_map/ppermute | solution.py:311
  108.9 12.6 %collective-permute-start.35 = (bf16[2,176,512]{2,1,0:T(8,128)(2,1)S(1)}, bf16[2,176,512]{2,1,0:T(8,128)(2,1)S(1)}, u32[]{:S(2)}, u32[]{:S(2)}) collective-permute-start(bf16[2,176,512]{2,1,0:T(8,128)(2,1)S(1)} %shard_map.91), channel_id=1, source_target_pairs={{4,8},{8,4},{5,9},{9,5},{6,10},{10,6},{7,11},{11,7},{20,24},{24,20... | collective-permute-start | bytes 1081352 | tf_op jit(solution)/shard_map/ppermute | solution.py:287
  117.6 21.9 %collective-permute-start.23 = (bf16[2,128,1024]{2,1,0:T(8,128)(2,1)S(1)}, bf16[2,128,1024]{2,1,0:T(8,128)(2,1)S(1)}, u32[]{:S(2)}, u32[]{:S(2)}) collective-permute-start(bf16[2,128,1024]{2,1,0:T(8,128)(2,1)S(1)} %get-tuple-element.30), channel_id=1, source_target_pairs={{0,1},{1,0},{2,3},{3,2},{4,5},{5,4},{6,7},{7,6},{8,9},{9,8},{10,11... | collective-permute-start | bytes 1572872 | tf_op jit(solution)/shard_map/ppermute | solution.py:311
  119.3 20.4 %collective-permute-start.30 = (bf16[128,1024]{1,0:T(8,128)(2,1)S(1)}, bf16[128,1024]{1,0:T(8,128)(2,1)S(1)}, u32[]{:S(2)}, u32[]{:S(2)}) collective-permute-start(bf16[128,1024]{1,0:T(8,128)(2,1)S(1)} %get-tuple-element.36), channel_id=1, source_target_pairs={{0,16},{16,0},{1,17},{17,1},{2,18},{18,2},{3,19},{19,3},{4,20},{20... | collective-permute-start | bytes 786440 | tf_op jit(solution)/shard_map/ppermute | solution.py:335
  120.9 20.4 %collective-permute-start.28 = (bf16[128,1024]{1,0:T(8,128)(2,1)S(1)}, bf16[128,1024]{1,0:T(8,128)(2,1)S(1)}, u32[]{:S(2)}, u32[]{:S(2)}) collective-permute-start(bf16[128,1024]{1,0:T(8,128)(2,1)S(1)} %get-tuple-element.34), channel_id=1, source_target_pairs={{0,16},{16,0},{1,17},{17,1},{2,18},{18,2},{3,19},{19,3},{4,20},{20... | collective-permute-start | bytes 786440 | tf_op jit(solution)/shard_map/ppermute | solution.py:335
  121.4 14.1 %collective-permute-start.40 = (bf16[176,512]{1,0:T(8,128)(2,1)S(1)}, bf16[176,512]{1,0:T(8,128)(2,1)S(1)}, u32[]{:S(2)}, u32[]{:S(2)}) collective-permute-start(bf16[176,512]{1,0:T(8,128)(2,1)S(1)} %shard_map.95), channel_id=1, source_target_pairs={{0,4},{4,0},{8,12},{12,8},{1,5},{5,1},{9,13},{13,9},{2,6},{6,2},{1... | collective-permute-start | bytes 540680 | tf_op jit(solution)/shard_map/ppermute | solution.py:318
  139.8 11.9 %collective-permute-start.31 = (bf16[128,1024]{1,0:T(8,128)(2,1)S(1)}, bf16[128,1024]{1,0:T(8,128)(2,1)S(1)}, u32[]{:S(2)}, u32[]{:S(2)}) collective-permute-start(bf16[128,1024]{1,0:T(8,128)(2,1)S(1)} %shard_map.88.a), channel_id=1, source_target_pairs={{0,2},{2,0},{1,3},{3,1},{4,6},{6,4},{5,7},{7,5},{8,10},{10,8},{9,1... | collective-permute-start | bytes 786440 | tf_op jit(solution)/shard_map/ppermute | solution.py:337
  (26 other events, 220.5 us)
